TPU v7x, 32 devices: a whole 2x2x4 slice. The times are simulated.
32 devices in a mesh: rep: 2 (over x), fs: 8 (over z, y), tp: 2 (over core).
Axes of the slice: x: 2, y: 2, z: 4, core: 2. Of those that a mesh axis runs over, the one named last changes fastest.
Arguments:
- x_late: bfloat16 [2048, 2048], P(('rep', 'fs')), parts along dimension 0, may hold values from -6 to 6
- x_early: bfloat16 [2048, 2048], P(('rep', 'fs')), parts along dimension 0, may hold values from -6 to 6
- cotangent: bfloat16 [2048, 2048], P(('rep', 'fs')), parts along dimension 0, may hold values from -6 to 6
- pre_gain: float32 [2048], replicated, may hold values from 0.1 to 1.9
- post_gain: float32 [2048], replicated, may hold values from 0.1 to 1.9
- gate_weight: bfloat16 [2048, 3072], P('fs', 'tp'), may hold values from -0.125 to 0.125
- up_weight: bfloat16 [2048, 3072], P('fs', 'tp'), may hold values from -0.125 to 0.125
- down_weight: bfloat16 [2048, 3072], P('fs', 'tp'), may hold values from -0.109375 to 0.109375
- down_grad_sum: float32 [4096, 3072], P(('rep', 'fs'), 'tp'), parts along dimension 0, may hold values from -6 to 6
Outputs:
- y_late: bfloat16 [2048, 2048], P(('rep', 'fs')), parts along dimension 0
- dx_early: bfloat16 [2048, 2048], P(('rep', 'fs')), parts along dimension 0
- down_grad_out: float32 [4096, 3072], P(('rep', 'fs'), 'tp'), parts along dimension 0
There are 2 independent parts, one for each index of `rep`. A program takes and returns all parts, laid end to end along the dimension named above; an argument that names none is the same for every part. Nothing has to cross between parts.
All inputs are finite; a program needn't handle non-finite values.
Results may differ from a plain program's by a relative error of at most 0.023.
Values may be sent and summed in bfloat16 or wider, within the bound.
A program may use at most 64 MiB of HBM per device.

v0:
```python
import jax
import jax.numpy as jnp
from jax import lax
from jax.sharding import PartitionSpec as P

eps = 1e-06


def pre_norm(x, pre_gain):
    xf = x.astype(jnp.float32)
    scale = lax.rsqrt(jnp.mean(xf * xf, axis=-1, keepdims=True) + eps)
    return (xf, scale, (xf * scale * pre_gain).astype(jnp.bfloat16))


def right_product(left, right):
    return lax.dot_general(
        left, right, (((1,), (1,)), ((), ())), preferred_element_type=jnp.float32
    )


def body(
    x_late,
    x_early,
    cotangent,
    pre_gain,
    post_gain,
    gate_weight,
    up_weight,
    down_weight,
    down_grad_sum,
):
    rows = x_late.shape[0]
    late_f, late_rs, late_norm = pre_norm(x_late, pre_gain)
    early_f, early_rs, early_norm = pre_norm(x_early, pre_gain)
    normed = jnp.concatenate([late_norm, early_norm], axis=0)
    pieces = (
        lax.all_gather(gate_weight, "fs", axis=0, tiled=True),
        lax.all_gather(up_weight, "fs", axis=0, tiled=True),
    )
    columns = normed
    gate = jnp.dot(columns, pieces[0], preferred_element_type=jnp.float32)
    up = jnp.dot(columns, pieces[1], preferred_element_type=jnp.float32)
    hidden = (jax.nn.silu(gate) * up).astype(jnp.bfloat16)
    partial_value = right_product(hidden, lax.all_gather(down_weight, "fs", axis=0, tiled=True))
    branch = lax.psum(partial_value.astype(jnp.bfloat16), "tp").astype(jnp.float32)
    branch_l = branch[:rows]
    branch_e = branch[rows:]
    late_rz = lax.rsqrt(jnp.mean(branch_l * branch_l, axis=-1, keepdims=True) + eps)
    y_late = (late_f + 0.5 * branch_l * late_rz * post_gain).astype(jnp.bfloat16)
    early_rz = lax.rsqrt(jnp.mean(branch_e * branch_e, axis=-1, keepdims=True) + eps)
    cot_f = cotangent.astype(jnp.float32)
    dpost = 0.5 * cot_f * post_gain
    dbranch = early_rz * (
        dpost - branch_e * early_rz * early_rz * jnp.mean(branch_e * dpost, axis=-1, keepdims=True)
    )
    dbranch = dbranch.astype(jnp.bfloat16)
    columns = dbranch
    dhidden = jnp.dot(
        columns,
        lax.all_gather(down_weight, "fs", axis=0, tiled=True),
        preferred_element_type=jnp.float32,
    )
    gate_e = gate[rows:]
    up_e = up[rows:]
    sig = jax.nn.sigmoid(gate_e)
    dgate = (dhidden * up_e * sig * (1.0 + gate_e * (1.0 - sig))).astype(jnp.bfloat16)
    dup = (dhidden * gate_e * sig).astype(jnp.bfloat16)
    pieces = lax.all_gather((gate_weight, up_weight), "fs", axis=0, tiled=True)
    dpartial = right_product(dgate, pieces[0]) + right_product(dup, pieces[1])
    dnormed = lax.psum(dpartial.astype(jnp.bfloat16), "tp").astype(jnp.float32)
    gained = pre_gain * dnormed
    dx_early = cot_f + early_rs * (
        gained - early_f * early_rs * early_rs * jnp.mean(early_f * gained, axis=-1, keepdims=True)
    )
    dx_early = dx_early.astype(jnp.bfloat16)
    hidden_e = hidden[rows:]
    owned = lax.all_to_all(dbranch, "fs", split_axis=1, concat_axis=0, tiled=True)
    summed = lax.dot_general(
        owned,
        lax.all_gather(hidden_e, "fs", axis=0, tiled=True),
        (((0,), (0,)), ((), ())),
        preferred_element_type=jnp.float32,
    )
    down_grad_out = down_grad_sum + summed
    return (y_late, dx_early, down_grad_out)


def solution(mesh):
    in_specs = (
        P(("rep", "fs"), None),
        P(("rep", "fs"), None),
        P(("rep", "fs"), None),
        P(),
        P(),
        P("fs", "tp"),
        P("fs", "tp"),
        P("fs", "tp"),
        P(("rep", "fs"), "tp"),
    )
    out_specs = (P(("rep", "fs"), None), P(("rep", "fs"), None), P(("rep", "fs"), "tp"))
    return jax.shard_map(body, mesh=mesh, in_specs=in_specs, out_specs=out_specs, check_vma=False)
```

profile of v0, /device:TPU:0, one launch (start us, length us, event | category | flops | bytes accessed | tf_op | source)
XLA Modules:
  0.0 441.1 jit_solution(18082639980764139476)
XLA Ops:
  7.2 0.7 all-gather.5.cloned.1.call-update
  8.0 0.7 all-gather.7.cloned.1.call-update
  10.2 101.4 %all-gather.5.cloned.1.call-done = bf16[2048,1536]{1,0:T(8,128)(2,1)} async-done(((bf16[256,1536]{1,0:T(8,128)(2,1)}), bf16[2048,1536]{1,0:T(8,128)(2,1)}) %all-gather.5.cloned.1.call-update) | async-done | bytes 6291472 | tf_op jit(solution)/shard_map/all_gather | solution.py:37
  111.6 5.7 %fusion.23 = f32[256,1536]{1,0:T(8,128)} fusion(bf16[2048,1536]{1,0:T(8,128)(2,1)} %all-gather.5.cloned.1.call-done, bf16[128,2048]{1,0:T(8,128)(2,1)S(1)} %get-tuple-element.9, bf16[128,2048]{1,0:T(8,128)(2,1)S(1)} %get-tuple-element.8), kind=kOutput, calls=%fused_computation.42 | convolution fusion | flops 1612709888 | bytes 8912896 | tf_op jit(solution)/shard_map/dot_general | solution.py:41
  117.4 93.4 %all-gather.7.cloned.1.call-done = bf16[2048,1536]{1,0:T(8,128)(2,1)} async-done(((bf16[256,1536]{1,0:T(8,128)(2,1)}), bf16[2048,1536]{1,0:T(8,128)(2,1)}) %all-gather.7.cloned.1.call-update) | async-done | bytes 6291472 | tf_op jit(solution)/shard_map/all_gather | solution.py:38
  210.7 6.2 %multiply_convert_fusion = (bf16[256,1536]{1,0:T(8,128)(2,1)S(1)}, f32[256,1536]{1,0:T(8,128)}) fusion(f32[256,1536]{1,0:T(8,128)} %fusion.23, bf16[2048,1536]{1,0:T(8,128)(2,1)} %all-gather.7.cloned.1.call-done, bf16[128,2048]{1,0:T(8,128)(2,1)S(1)} %get-tuple-element.9, bf16[128,2048]{1,0:T(8,128)(2,1)S(1)} %get-tuple-element.8), kind=kOutput, calls=%fused_computation.4 | convolution fusion | flops 1615069184 | bytes 11272192 | tf_op jit(solution)/shard_map/dot_general | solution.py:42
  216.9 92.9 %all-gather.9.cloned.1.call-done = bf16[2048,1536]{1,0:T(8,128)(2,1)} async-done(((bf16[256,1536]{1,0:T(8,128)(2,1)}), bf16[2048,1536]{1,0:T(8,128)(2,1)}) %all-gather.9.cloned.1.call-update) | async-done | bytes 6291472 | tf_op jit(solution)/shard_map/all_gather | solution.py:44
  309.8 5.6 %convolution_convert_fusion = bf16[256,2048]{1,0:T(8,128)(2,1)} fusion(bf16[256,1536]{1,0:T(8,128)(2,1)S(1)} %get-tuple-element.10, bf16[2048,1536]{1,0:T(8,128)(2,1)} %all-gather.9.cloned.1.call-done), kind=kOutput, calls=%fused_computation.1 | convolution fusion | flops 1611137024 | bytes 8126464 | tf_op jit(solution)/shard_map/dot_general | solution.py:16
  315.5 17.7 %all-reduce.3.cloned.1.call-done = bf16[256,2048]{1,0:T(8,128)(2,1)} async-done(((bf16[256,2048]{1,0:T(8,128)(2,1)}), bf16[256,2048]{1,0:T(8,128)(2,1)}) %all-reduce.3.cloned.1.call-update) | async-done | bytes 1048592 | tf_op jit(solution)/shard_map/psum | solution.py:45
  333.2 1.5 convert_element_type.51
  335.1 1.1 fusion.11
  336.2 1.4 copy-done
  337.7 1.0 fusion.32
  339.8 1.9 slice-done.1
  341.8 2.1 fusion.24
  344.0 3.0 fusion
  347.0 0.8 slice.24
  347.8 0.8 copy.15
  348.6 5.9 %all-to-all-start = ((bf16[128,8,256]{2,0,1:T(8,128)(2,1)}), bf16[128,8,256]{2,0,1:T(8,128)(2,1)S(1)}, u32[]{:S(2)}, u32[]{:S(2)}) async-start(bf16[128,8,256]{2,0,1:T(8,128)(2,1)} %bitcast.16), calls=%async_computation | async-start | bytes 1048576 | tf_op jit(solution)/shard_map/all_to_all | solution.py:77
  354.6 12.3 %all-reduce.5.cloned.1.call-done = bf16[128,2048]{1,0:T(8,128)(2,1)} async-done(((bf16[128,2048]{1,0:T(8,128)(2,1)}), bf16[128,2048]{1,0:T(8,128)(2,1)}) %all-reduce.5.cloned.1.call-update) | async-done | bytes 524304 | tf_op jit(solution)/shard_map/psum | solution.py:70
  366.9 1.3 fusion.18
  368.2 2.3 fusion.12
  370.5 59.7 %all-gather.11.cloned.1.call-done = bf16[1024,1536]{1,0:T(8,128)(2,1)} async-done(((bf16[128,1536]{1,0:T(8,128)(2,1)}), bf16[1024,1536]{1,0:T(8,128)(2,1)}) %all-gather.11.cloned.1.call-update) | async-done | bytes 3145744 | tf_op jit(solution)/shard_map/all_gather | solution.py:80
  430.2 4.0 convolution_add_fusion
  (47 shorter events, 3.3 us)
Async XLA Ops:
  7.2 2.3 copy-start.2
  7.2 2.5 copy-start.1
  7.2 2.7 copy-start.5
  7.2 104.4 %all-gather.5.cloned.1.call-start = ((), (), s32[]{:S(2)}) async-start(), calls=%async_computation.1 | async-start | bytes 7077888 | tf_op jit(solution)/shard_map/all_gather | solution.py:37
  7.9 202.8 %all-gather.7.cloned.1.call-start = ((), (), s32[]{:S(2)}) async-start(), calls=%async_computation.2 | async-start | bytes 7077888 | tf_op jit(solution)/shard_map/all_gather | solution.py:38
  8.7 301.1 %all-gather.9.cloned.1.call-start = ((), (), s32[]{:S(2)}) async-start(), calls=%async_computation.3 | async-start | bytes 7077888 | tf_op jit(solution)/shard_map/all_gather | solution.py:44
  9.4 323.8 %all-reduce.3.cloned.1.call-start = ((), (), s32[]{:S(2)}) async-start(), calls=%async_computation.4 | async-start | bytes 2097152 | tf_op jit(solution)/shard_map/psum | solution.py:45
  309.8 5.7 %copy-start.6 = (f32[2048]{0:T(1024)S(1)}, f32[2048]{0:T(1024)}, u32[]{:S(2)}) copy-start(f32[2048]{0:T(1024)} %param.13) | copy-start | bytes 24580
  315.4 19.2 %copy-start.3 = (bf16[128,2048]{1,0:T(8,128)(2,1)S(1)}, bf16[128,2048]{1,0:T(8,128)(2,1)}, u32[]{:S(2)}) copy-start(bf16[128,2048]{1,0:T(8,128)(2,1)} %param.11) | copy-start | bytes 1572868
  315.5 51.4 %all-reduce.5.cloned.1.call-start = ((), (), s32[]{:S(2)}) async-start(), calls=%async_computation.5 | async-start | bytes 1048576 | tf_op jit(solution)/shard_map/psum | solution.py:70
  334.7 3.0 copy-start
  335.1 3.9 slice-start
  335.1 4.3 copy-start.7
  335.1 4.7 %copy-start.8 = (f32[256,1536]{1,0:T(8,128)S(1)}, f32[256,1536]{1,0:T(8,128)}, u32[]{:S(2)}) copy-start(f32[256,1536]{1,0:T(8,128)} %get-tuple-element.11) | copy-start | bytes 4718596
  335.1 8.8 %slice-start.2 = ((s8[6291456]{0:T(1024)(128)(4,1)}), s8[4194304]{0:T(1024)(128)(4,1)S(1)}, s32[]{:S(2)}) async-start(s8[6291456]{0:T(1024)(128)(4,1)} %bitcast.21), calls=%async_computation.9 | async-start | bytes 8388608
  337.7 4.1 slice-start.1
  337.7 6.3 %slice-start.3 = ((s8[6291456]{0:T(1024)(128)(4,1)}), s8[2097152]{0:T(1024)(128)(4,1)S(1)}, s32[]{:S(2)}) async-start(s8[6291456]{0:T(1024)(128)(4,1)} %bitcast.21), calls=%async_computation.10 | async-start | bytes 4194304
  347.0 83.2 %all-gather.11.cloned.1.call-start = ((), (), s32[]{:S(2)}) async-start(), calls=%async_computation.6 | async-start | bytes 3538944 | tf_op jit(solution)/shard_map/all_gather | solution.py:80
  348.6 81.6 %copy-start.4 = (f32[256,1536]{1,0:T(8,128)S(1)}, f32[256,1536]{1,0:T(8,128)}, u32[]{:S(2)}) copy-start(f32[256,1536]{1,0:T(8,128)} %param.17) | copy-start | bytes 4718596
  348.6 21.8 %all-to-all-start = ((bf16[128,8,256]{2,0,1:T(8,128)(2,1)}), bf16[128,8,256]{2,0,1:T(8,128)(2,1)S(1)}, u32[]{:S(2)}, u32[]{:S(2)}) async-start(bf16[128,8,256]{2,0,1:T(8,128)(2,1)} %bitcast.16), calls=%async_computation | async-start | bytes 1048576 | tf_op jit(solution)/shard_map/all_to_all | solution.py:77
Sparse Core Ops, SparseCore 0:
  10.2 101.4 all-gather.4
  113.8 96.8 all-gather.6
  212.9 96.8 all-gather.8
  315.6 17.5 all-reduce.2
  347.1 19.7 all-reduce.4
  368.9 61.2 all-gather.10
where the time goes:
time: 442 us; the launch traced here: 441 us
  waiting for transfers between devices  380 us (86%)
  matrix products  27.7 us (6%)
  between operations  14.3 us (3%)
  other arithmetic  7.18 us (2%)
  local copies, waits for them, and re-layouts  6.17 us (1%)
  starting transfers between devices  6.17 us (1%)
    all_gather x1, waiting for transfers between devices, body(): lax.all_gather(gate_weight, 'fs', axis=0, tiled=True)  101 us
    all_gather x1, waiting for transfers between devices, body(): lax.all_gather(up_weight, 'fs', axis=0, tiled=True)  93.4 us
    all_gather x1, waiting for transfers between devices, body(): lax.all_gather(down_weight, 'fs', axis=0, tiled=True)  92.9 us
    all_gather x1, waiting for transfers between devices, body(): lax.all_gather(hidden_e, 'fs', axis=0, tiled=True)  59.7 us
    psum x1, waiting for transfers between devices, body(): lax.psum(partial_value.astype(jnp.bfloat16), 'tp').astype(jnp.float32)  17.7 us
    psum x1, waiting for transfers between devices, body(): dnormed = lax.psum(dpartial.astype(jnp.bfloat16), 'tp').astype(jnp.float32)  12.3 us
    dot_general x3, matrix products, right_product(): lax.dot_general(left, right, (((1,), (1,)), ((), ())), preferred_element_...  10.7 us
  transfers between devices with their start and end apart: 7, of which 6 were waited for; matrix products, arithmetic and copies ran while one was open for 4% of the time, Pallas kernels for 0%

commit v1 on v0

v1 whole, which is shorter than its diff:
```python
import functools
import itertools

import jax
import jax.numpy as jnp
from jax import lax
from jax.experimental import pallas as pl
from jax.experimental.pallas import tpu as pltpu
from jax.sharding import PartitionSpec as P

eps = 1e-06
F32, BF16 = jnp.float32, jnp.bfloat16
VMEM = pl.BlockSpec(memory_space=pltpu.VMEM)
DMA = pltpu.SemaphoreType.DMA


class Grid:
    def __init__(self, sizes):
        self.R, self.fs, self.tp = sizes
        self.fy = 2
        self.fz = self.fs // self.fy
        self.G = self.R * self.fy
        self.offsets = list(itertools.product(range(self.R), range(self.fy)))[1:]
        self.r, f, self.k = (lax.axis_index(n) for n in ("rep", "fs", "tp"))
        self.z, self.y = lax.div(f, self.fy), lax.rem(f, self.fy)
        self.g = self.r * self.fy + self.y

    def moved(self, o, sign=1):
        dr, dy = self.offsets[o]
        r = lax.rem(self.r + self.R + sign * dr, self.R)
        y = lax.rem(self.y + self.fy + sign * dy, self.fy)
        return r, y

    def index(self, o, sign=1):
        r, y = self.moved(o, sign)
        return r * self.fy + y

    def peer(self, o):
        r, y = self.moved(o)
        return {"rep": r, "fs": self.z * self.fy + y, "tp": self.k}

    def sibling_index(self, j):
        return lax.rem(self.k + j, self.tp)

    def sibling(self, j):
        return {"rep": self.r, "fs": self.z * self.fy + self.y, "tp": self.sibling_index(j)}

    def along(self, step):
        return lax.rem(self.z + self.fz + step, self.fz)

    def level(self, step):
        return {"rep": self.r, "fs": self.along(step) * self.fy + self.y, "tp": self.k}

    def barrier(self, group=False, pair=False, ring=False, levels=False):
        sem = pltpu.get_barrier_semaphore()
        targets = []
        if group:
            targets += [self.peer(o) for o in range(len(self.offsets))]
        if pair:
            targets += [self.sibling(j) for j in range(1, self.tp)]
        if levels:
            targets += [self.level(s) for s in range(1, self.fz)]
        elif ring:
            targets += [self.level(1), self.level(-1)]
        for t in targets:
            pl.semaphore_signal(sem, inc=1, device_id=t, device_id_type=pl.DeviceIdType.MESH)
        pl.semaphore_wait(sem, len(targets))


def push(src, dst, send, recv, to):
    copy = pltpu.make_async_remote_copy(
        src_ref=src, dst_ref=dst, send_sem=send, recv_sem=recv,
        device_id=to, device_id_type=pl.DeviceIdType.MESH,
    )
    copy.start()
    return copy


def ring_start(m, first, slot, sems, chunks):
    half, sent = m.fz // 2, {}
    orders = {0: list(range(chunks)), 1: list(range(chunks))[chunks // 2:] + list(range(chunks // 2))}

    def send(d, s, c):
        sign = 1 if d == 0 else -1
        block = m.along(-sign * (s - 1))
        src = first(c) if s == 1 else slot(block, c)
        i = (d * half + s - 1) * chunks + c
        sent[d, s, c] = push(src, slot(block, c), sems.at[0, i], sems.at[1, i], m.level(sign))

    return orders, send, sent


def ring_travels(m, d, s, c, chunks):
    half = m.fz // 2
    return s < half or (c < chunks // 2) == (d == 0)


def ring_rest(m, orders, send, sent, chunks):
    half = m.fz // 2
    waited = set()
    for s in range(2, half + 1):
        for i in range(chunks):
            for d in (0, 1):
                c = orders[d][i]
                if ring_travels(m, d, s, c, chunks):
                    sent[d, s - 1, c].wait_recv()
                    waited.add((d, s - 1, c))
                    send(d, s, c)

    def finish():
        for key, copy in sent.items():
            copy.wait_send()
            if key not in waited:
                copy.wait_recv()

    return finish


def group_gather_start(m, x, out, sems):
    return [
        push(x.at[m.k], out.at[m.g, m.k], sems.at[0, o], sems.at[1, o], m.peer(o))
        for o in range(len(m.offsets))
    ]


def group_gather_finish(m, copies, out, sems):
    n, passed = len(m.offsets), []
    for o, copy in enumerate(copies):
        copy.wait_recv()
        src = m.index(o, -1)
        for j in range(1, m.tp):
            i = n + o * (m.tp - 1) + j - 1
            passed.append(
                push(out.at[src, m.k], out.at[src, m.k], sems.at[0, i], sems.at[1, i], m.sibling(j))
            )
    for copy in copies:
        copy.wait_send()
    for copy in passed:
        copy.wait()


def first_kernel(sizes, w, x, wout, xout, ysem, zsem, gsem):
    m = Grid(sizes)
    m.barrier(group=True, pair=True, ring=True)
    f = m.z * m.fy + m.y
    nw = w.shape[1]
    chunks = m.fy * nw

    def where(z, c):
        e, i = divmod(c, nw)
        return wout.at[i, z * m.fy + lax.rem(m.y + e, m.fy)]

    def first(c):
        return w.at[m.g, c] if c < nw else where(m.z, c)

    ycopies = {}
    for i in range(nw):
        for e in range(1, m.fy):
            o = m.offsets.index((0, e))
            j = (e - 1) * nw + i
            ycopies[e, i] = push(w.at[m.index(o), i], wout.at[i, f], ysem.at[0, j], ysem.at[1, j], m.peer(o))
    orders, send, sent = ring_start(m, first, where, zsem, chunks)
    for c in range(nw):
        send(0, 1, c)
        send(1, 1, c)
    gathered = group_gather_start(m, x, xout, gsem)
    for i in range(nw):
        wout[i, f] = w[m.g, i]
    xout[m.g] = x[...]
    for c in range(nw, chunks):
        e, i = divmod(c, nw)
        back = (m.fy - e) % m.fy
        ycopies[back, i].wait_recv()
        send(0, 1, c)
        send(1, 1, c)
    group_gather_finish(m, gathered, xout, gsem)
    finish = ring_rest(m, orders, send, sent, chunks)
    finish()
    for copy in ycopies.values():
        copy.wait_send()


def scatter_start(m, p, rx, sems):
    n = len(m.offsets)
    copies = {}
    for o in list(range(n)) + [n]:
        block = m.g if o == n else m.index(o)
        for j in range(1, m.tp):
            i = o * (m.tp - 1) + j - 1
            copies[o, j] = push(
                p.at[block, m.sibling_index(j)], rx.at[j - 1, o], sems.at[0, i], sems.at[1, i], m.sibling(j)
            )
    return copies


def scatter_rest(m, p, out, rx, tx, rg, copies, sems, fill=lambda: None):
    n = len(m.offsets)
    base = (n + 1) * (m.tp - 1)

    def total(o):
        block = m.g if o == n else m.index(o)
        value = p[block, m.k].astype(F32)
        for j in range(1, m.tp):
            copies[o, j].wait_recv()
            value = value + rx[j - 1, o].astype(F32)
        return value

    sends = []
    for o in range(n):
        tx[o] = total(o).astype(BF16)
        sends.append(push(tx.at[o], rg.at[o], sems.at[0, base + o], sems.at[1, base + o], m.peer(o)))
    out[m.k] = total(n)
    fill()
    for o in range(n):
        sends[o].wait_recv()
        out[m.k] = out[m.k] + rg[o].astype(F32)
    passed = []
    for j in range(1, m.tp):
        i = base + n + j - 1
        passed.append(push(out.at[m.k], out.at[m.k], sems.at[0, i], sems.at[1, i], m.sibling(j)))
    for copy in copies.values():
        copy.wait_send()
    for copy in sends:
        copy.wait_send()
    for copy in passed:
        copy.wait()


def branch_kernel(sizes, p, h, out, hout, rx, tx, rg, sems, zsem):
    m = Grid(sizes)
    m.barrier(group=True, pair=True, ring=True)
    copies = scatter_start(m, p, rx, sems)
    chunks = m.G
    orders, send, sent = ring_start(m, lambda c: h.at[c], lambda z, c: hout.at[z, c], zsem, chunks)
    for i in range(chunks):
        for d in (0, 1):
            send(d, 1, orders[d][i])

    ends = []

    def fill():
        hout[m.z] = h[...]
        ends.append(ring_rest(m, orders, send, sent, chunks))

    scatter_rest(m, p, out, rx, tx, rg, copies, sems, fill)
    ends[0]()


def gather_kernel(sizes, x, out, sems):
    m = Grid(sizes)
    m.barrier(group=True, pair=True)
    copies = group_gather_start(m, x, out, sems)
    out[m.g] = x[...]
    group_gather_finish(m, copies, out, sems)


def back_kernel(sizes, p, d, out, dout, rx, tx, rg, sems, zsem):
    m = Grid(sizes)
    m.barrier(group=True, pair=True, levels=True)
    copies = scatter_start(m, p, rx, sems)
    steps = list(range(1, m.fz))
    across = {}
    for s in steps:
        across[s] = push(
            d.at[m.along(s), m.k], dout.at[m.z, m.k], zsem.at[0, s - 1], zsem.at[1, s - 1], m.level(s)
        )
    passed = []

    def fill():
        dout[m.z] = d[m.z]

    scatter_rest(m, p, out, rx, tx, rg, copies, sems, fill)
    for s in steps:
        across[s].wait_recv()
        src = m.along(-s)
        for j in range(1, m.tp):
            i = len(steps) + (s - 1) * (m.tp - 1) + j - 1
            passed.append(push(dout.at[src, m.k], dout.at[src, m.k], zsem.at[0, i], zsem.at[1, i], m.sibling(j)))
    for s in steps:
        across[s].wait_send()
    for copy in passed:
        copy.wait()


def exchange_kernel(sizes, w, out, sems):
    m = Grid(sizes)
    m.barrier(group=True)
    copies = [
        push(w.at[m.index(o)], out.at[m.g], sems.at[0, o], sems.at[1, o], m.peer(o))
        for o in range(len(m.offsets))
    ]
    out[m.g] = w[m.g]
    for copy in copies:
        copy.wait()


def call(kernel, sizes, ident, outs, scratch, *args):
    size = sum(a.size * a.dtype.itemsize for a in list(args) + list(outs))
    return pl.pallas_call(
        functools.partial(kernel, sizes),
        out_shape=outs,
        in_specs=[VMEM] * len(args),
        out_specs=[VMEM] * len(outs),
        scratch_shapes=scratch,
        compiler_params=pltpu.CompilerParams(
            collective_id=ident, has_side_effects=True, vmem_limit_bytes=56 * 1024 * 1024
        ),
        cost_estimate=pl.CostEstimate(flops=0, bytes_accessed=size, transcendentals=0),
    )(*args)


def pre_norm(x, pre_gain):
    xf = x.astype(F32)
    scale = lax.rsqrt(jnp.mean(xf * xf, axis=-1, keepdims=True) + eps)
    return (xf, scale, (xf * scale * pre_gain).astype(BF16))


def right_product(left, right):
    return lax.dot_general(left, right, (((1,), (1,)), ((), ())), preferred_element_type=F32)


def body(sizes, x_late, x_early, cotangent, pre_gain, post_gain, gate_weight, up_weight, down_weight,
         down_grad_sum):
    R, fs, tp = sizes
    fy = 2
    fz, G = fs // fy, R * fy
    rows, D = x_late.shape
    drows, width = gate_weight.shape
    part = width // G
    n = G - 1
    S = jax.ShapeDtypeStruct

    late_f, late_rs, late_norm = pre_norm(x_late, pre_gain)
    early_f, early_rs, early_norm = pre_norm(x_early, pre_gain)
    normed = jnp.concatenate([late_norm, early_norm], axis=0)
    c = 2 * rows // tp
    weights = jnp.stack([w.reshape(drows, G, part) for w in (gate_weight, up_weight, down_weight)])
    weights = weights.transpose(2, 0, 1, 3)
    ring = fz // 2
    wall, xall = call(
        first_kernel, sizes, 0,
        [S((3, fs, drows, part), BF16), S((G, tp, c, D), BF16)],
        [DMA((2, 3 * (fy - 1))), DMA((2, 2 * ring * 3 * fy)), DMA((2, n + n * (tp - 1)))],
        weights, normed.reshape(tp, c, D),
    )
    wall = wall.reshape(3, D, part)
    xall = xall.reshape(G * 2 * rows, D)
    gate = jnp.dot(xall, wall[0], preferred_element_type=F32)
    up = jnp.dot(xall, wall[1], preferred_element_type=F32)
    hidden = (jax.nn.silu(gate) * up).astype(BF16)
    partial_value = right_product(hidden, wall[2]).astype(BF16).reshape(G, tp, c, D)
    early_of = lambda a: a.reshape(G, 2, rows, part)[:, 1]
    hidden_e = early_of(hidden)

    def scatter_scratch(c):
        return [
            pltpu.VMEM((tp - 1, n + 1, c, D), BF16),
            pltpu.VMEM((n, c, D), BF16),
            pltpu.VMEM((n, c, D), BF16),
            DMA((2, (n + 1) * (tp - 1) + n + tp - 1)),
        ]

    branch, hall = call(
        branch_kernel, sizes, 1,
        [S((tp, c, D), F32), S((fz, G, rows, part), BF16)],
        scatter_scratch(c) + [DMA((2, 2 * ring * G))],
        partial_value, hidden_e,
    )
    branch = branch.reshape(2 * rows, D)
    branch_l, branch_e = branch[:rows], branch[rows:]
    late_rz = lax.rsqrt(jnp.mean(branch_l * branch_l, axis=-1, keepdims=True) + eps)
    y_late = (late_f + 0.5 * branch_l * late_rz * post_gain).astype(BF16)
    early_rz = lax.rsqrt(jnp.mean(branch_e * branch_e, axis=-1, keepdims=True) + eps)
    cot_f = cotangent.astype(F32)
    dpost = 0.5 * cot_f * post_gain
    dbranch = early_rz * (
        dpost - branch_e * early_rz * early_rz * jnp.mean(branch_e * dpost, axis=-1, keepdims=True)
    )
    ce = rows // tp
    (dall,) = call(
        gather_kernel, sizes, 2,
        [S((G, tp, ce, D), BF16)],
        [DMA((2, n + n * (tp - 1)))],
        dbranch.astype(BF16).reshape(tp, ce, D),
    )
    dall = dall.reshape(G * rows, D)
    dhidden = jnp.dot(dall, wall[2], preferred_element_type=F32)
    gate_e = early_of(gate).reshape(G * rows, part)
    up_e = early_of(up).reshape(G * rows, part)
    sig = jax.nn.sigmoid(gate_e)
    dgate = (dhidden * up_e * sig * (1.0 + gate_e * (1.0 - sig))).astype(BF16)
    dup = (dhidden * gate_e * sig).astype(BF16)
    dpartial = right_product(dgate, wall[0]) + right_product(dup, wall[1])
    dpartial = dpartial.astype(BF16).reshape(G, tp, ce, D)
    feats = D // fz
    spread = dall.reshape(tp, G * rows // tp, fz, feats).transpose(2, 0, 1, 3)
    dnormed, dfeat = call(
        back_kernel, sizes, 3,
        [S((tp, ce, D), F32), S((fz, tp, G * rows // tp, feats), BF16)],
        scatter_scratch(ce) + [DMA((2, (fz - 1) * tp))],
        dpartial, spread,
    )
    gained = pre_gain * dnormed.reshape(rows, D)
    dx_early = cot_f + early_rs * (
        gained - early_f * early_rs * early_rs * jnp.mean(early_f * gained, axis=-1, keepdims=True)
    )
    dx_early = dx_early.astype(BF16)
    dfeat = dfeat.reshape(fz, R, fy * rows, feats)
    hall = hall.reshape(fz, R, fy * rows, part)
    summed = jnp.stack([
        lax.dot_general(
            dfeat[:, r].reshape(fz * fy * rows, feats), hall[:, r].reshape(fz * fy * rows, part),
            (((0,), (0,)), ((), ())), preferred_element_type=F32,
        )
        for r in range(R)
    ])
    summed = summed.astype(BF16).reshape(G, drows, part)
    (owned,) = call(exchange_kernel, sizes, 4, [S((G, drows, part), BF16)], [DMA((2, n))], summed)
    owned = owned.transpose(1, 0, 2).reshape(drows, width)
    down_grad_out = down_grad_sum + owned.astype(F32)
    return (y_late, dx_early, down_grad_out)


def solution(mesh):
    sizes = tuple(mesh.shape[a] for a in ("rep", "fs", "tp"))
    in_specs = (
        P(("rep", "fs"), None),
        P(("rep", "fs"), None),
        P(("rep", "fs"), None),
        P(),
        P(),
        P("fs", "tp"),
        P("fs", "tp"),
        P("fs", "tp"),
        P(("rep", "fs"), "tp"),
    )
    out_specs = (P(("rep", "fs"), None), P(("rep", "fs"), None), P(("rep", "fs"), "tp"))
    return jax.shard_map(
        functools.partial(body, sizes), mesh=mesh, in_specs=in_specs, out_specs=out_specs, check_vma=False
    )
```

time: 442 us -> 246 us (0.56)
  waiting for transfers between devices: 380 us -> 0 us
  Pallas kernels: 0 us -> 186 us
  local copies, waits for them, and re-layouts: 6.17 us -> 22.5 us
  between operations: 14.3 us -> 0.96 us
  matrix products: 27.7 us -> 18.6 us
  other arithmetic: 7.18 us -> 15.5 us
  starting transfers between devices: 6.17 us -> 0 us
    all_gather x4 -> x0, waiting for transfers between devices: 347 us -> none  [the longest x1 101 us: body(): lax.all_gather(gate_weight, 'fs', axis=0, tiled=True)]
    pallas_call x0 -> x5, Pallas kernels: none -> 186 us  [call(): pl.pallas_call(functools.partial(kernel, sizes), out_shape=outs, in_specs...]
    psum x2 -> x0, waiting for transfers between devices: 30 us -> none  [the longest x1 17.7 us: body(): lax.psum(partial_value.astype(jnp.bfloat16), 'tp').astype(jnp.float32)]
    another operation x0 -> x5, local copies, waits for them, and re-layouts: none -> 7.14 us  [the longest x2 6.07 us: body(): spread = dall.reshape(tp, G * rows // tp, fz, feats).transpose(2, 0, 1, 3)]
    dot_general x4 -> x5, matrix products: 17 us -> 10.3 us  [the longest x1 3.51 us: body(): up = jnp.dot(xall, wall[1], preferred_element_type=F32)]
    all_to_all x1 -> x0, starting transfers between devices: 5.93 us -> none  [body(): lax.all_to_all(dbranch, 'fs', split_axis=1, concat_axis=0, tiled=True)]
    slice x1 -> x3, local copies, waits for them, and re-layouts: 0.77 us -> 5.65 us  [the longest x1 3.12 us: body(): wall[2]]
  transfers between devices with their start and end apart: 7 -> 0, of which waited for: 6 -> 0; matrix products, arithmetic and copies ran while one was open for 4% -> 0% of each run, Pallas kernels for 0% -> 0%
where the time goes in v1:
time: 246 us; the launch traced here: 243 us
  Pallas kernels  186 us (76%)
  local copies, waits for them, and re-layouts  22.5 us (9%)
  matrix products  18.6 us (8%)
  other arithmetic  15.5 us (6%)
    pallas_call x5, Pallas kernels, call(): pl.pallas_call(functools.partial(kernel, sizes), out_shape=outs, in_specs...  186 us
    unnamed x41, local copies, waits for them, and re-layouts  8.47 us
    dot_general x3, matrix products, right_product(): lax.dot_general(left, right, (((1,), (1,)), ((), ())), preferred_element_...  8.25 us
    another operation x2, local copies, waits for them, and re-layouts, body(): spread = dall.reshape(tp, G * rows // tp, fz, feats).transpose(2, 0, 1, 3)  6.07 us

profile of v1, /device:TPU:0, one launch (start us, length us, event | category | flops | bytes accessed | tf_op | source)
XLA Modules:
  0.0 243.3 jit_solution(9698099763040851249)
XLA Ops:
  3.1 1.5 fusion.18
  9.2 1.8 maximum_bitcast_fusion.w
  10.9 87.7 %shard_map.112 = (bf16[3,8,256,384]{3,2,1,0:T(8,128)(2,1)}, bf16[4,2,128,2048]{3,2,1,0:T(8,128)(2,1)}) custom-call(bf16[4,3,256,384]{3,2,1,0:T(8,128)(2,1)} %maximum_bitcast_fusion.w, bf16[2,128,2048]{2,1,0:T(8,128)(2,1)} %bitcast.141), custom_call_target="tpu_custom_call" | custom-call | bytes 12320768 | tf_op jit(solution)/shard_map/pallas_call | solution.py:299
  98.7 3.1 %fusion.40 = (bf16[1,8,256,384]{3,2,1,0:T(8,128)(2,1)S(1)}, bf16[1,8,256,384]{3,2,1,0:T(8,128)(2,1)S(1)}, bf16[1,8,256,384]{3,2,1,0:T(8,128)(2,1)S(1)}) fusion(bf16[3,8,256,384]{3,2,1,0:T(8,128)(2,1)} %get-tuple-element.10), kind=kLoop, calls=%fused_computation.78 | loop fusion | bytes 9437184 | tf_op jit(solution)/shard_map/slice | solution.py:351
  102.3 2.3 fusion.41
  104.6 3.5 %multiply_convert_fusion = (bf16[1024,384]{1,0:T(8,128)(2,1)S(1)}, f32[1024,384]{1,0:T(8,128)}) fusion(f32[1024,384]{1,0:T(8,128)S(1)} %fusion.41, bf16[1024,2048]{1,0:T(8,128)(2,1)S(1)} %bitcast.153, bf16[2048,384]{1,0:T(8,128)(2,1)S(1)} %bitcast.138), kind=kOutput, calls=%fused_computation.6 | convolution fusion | flops 1612972032 | bytes 9699328 | tf_op jit(solution)/shard_map/dot_general | solution.py:349
  108.1 4.3 %convolution_convert_fusion = bf16[1024,2048]{1,0:T(8,128)(2,1)} fusion(bf16[1024,384]{1,0:T(8,128)(2,1)S(1)} %get-tuple-element.30, bf16[2048,384]{1,0:T(8,128)(2,1)S(1)} %bitcast.147), kind=kOutput, calls=%fused_computation.1 | convolution fusion | flops 1612709888 | bytes 6553600 | tf_op jit(solution)/shard_map/dot_general | solution.py:319
  113.2 37.8 %shard_map.113 = (f32[2,128,2048]{2,1,0:T(8,128)}, bf16[4,4,128,384]{3,2,1,0:T(8,128)(2,1)}) custom-call(bf16[4,2,128,2048]{3,2,1,0:T(8,128)(2,1)} %bitcast.140, bf16[4,128,384]{2,1,0:T(8,128)(2,1)} %slice_bitcast_fusion.4.h), custom_call_target="tpu_custom_call" | custom-call | bytes 8257536 | tf_op jit(solution)/shard_map/pallas_call | solution.py:299
  151.1 2.1 fusion.24
  153.4 1.4 fusion.14
  154.8 18.6 %shard_map.114 = bf16[4,2,64,2048]{3,2,1,0:T(8,128)(2,1)} custom-call(bf16[2,64,2048]{2,1,0:T(8,128)(2,1)} %bitcast.146), custom_call_target="tpu_custom_call" | custom-call | bytes 2621440 | tf_op jit(solution)/shard_map/pallas_call | solution.py:299
  173.5 1.3 slice.63
  176.0 1.6 fusion.38
  177.7 1.3 fusion.42
  178.9 2.6 %add_convert_fusion = bf16[512,2048]{1,0:T(8,128)(2,1)} fusion(f32[512,2048]{1,0:T(8,128)S(1)} %fusion.42, bf16[512,384]{1,0:T(8,128)(2,1)S(1)} %get-tuple-element.26, bf16[2048,384]{1,0:T(8,128)(2,1)S(1)} %bitcast.139), kind=kOutput, calls=%fused_computation | convolution fusion | flops 807403520 | bytes 8257536 | tf_op jit(solution)/shard_map/dot_general | solution.py:319
  181.6 2.8 %reshape_reshape.3 = bf16[2,256,4,512]{3,2,1,0:T(4,128)(2,1)} reshape(bf16[4,2,64,2048]{3,2,1,0:T(8,128)(2,1)S(1)} %copy-done) | data formatting | bytes 4194304 | tf_op jit(solution)/shard_map/reshape;reshape | solution.py:396
  184.3 3.3 %copy.37 = bf16[2,256,4,512]{3,1,0,2:T(8,128)(2,1)} copy(bf16[2,256,4,512]{3,2,1,0:T(4,128)(2,1)} %reshape_reshape.3) | data formatting | bytes 4194304 | tf_op jit(solution)/shard_map/reshape;reshape | solution.py:396
  187.7 27.2 %shard_map.115 = (f32[2,64,2048]{2,1,0:T(8,128)}, bf16[4,2,256,512]{3,2,1,0:T(8,128)(2,1)}) custom-call(bf16[4,2,64,2048]{3,2,1,0:T(8,128)(2,1)} %bitcast.135, bf16[4,2,256,512]{3,2,1,0:T(8,128)(2,1)} %bitcast.134), custom_call_target="tpu_custom_call" | custom-call | bytes 7340032 | tf_op jit(solution)/shard_map/pallas_call | solution.py:299
  214.9 2.1 fusion.7
  218.7 14.4 %shard_map.116 = bf16[4,256,384]{2,1,0:T(8,128)(2,1)} custom-call(bf16[4,256,384]{2,1,0:T(8,128)(2,1)} %bitcast.142), custom_call_target="tpu_custom_call" | custom-call | bytes 1572864 | tf_op jit(solution)/shard_map/pallas_call | solution.py:299
  233.1 1.2 convert_bitcast_fusion
  234.8 3.0 %copy.29 = f32[256,1536]{0,1:T(8,128)} copy(f32[256,1536]{1,0:T(8,128)} %param.17) | data formatting | bytes 3145728 | tf_op args[8]
  237.8 1.6 bitcast_add_fusion
  239.4 1.6 copy.30
  (58 shorter events, 14.0 us)
Async XLA Ops:
  4.6 1.4 copy-start.9
  6.0 1.1 copy-start.10
  7.4 1.1 copy-start.11
  98.7 3.6 %copy-start.15 = (bf16[4,2,128,2048]{3,2,1,0:T(8,128)(2,1)S(1)}, bf16[4,2,128,2048]{3,2,1,0:T(8,128)(2,1)}, u32[]{:S(2)}) copy-start(bf16[4,2,128,2048]{3,2,1,0:T(8,128)(2,1)} %get-tuple-element.9) | copy-start | bytes 12582916
  101.8 6.3 %copy-start.7 = (bf16[1,8,256,384]{3,2,1,0:T(8,128)(2,1)}, bf16[1,8,256,384]{3,2,1,0:T(8,128)(2,1)S(1)}, u32[]{:S(2)}) copy-start(bf16[1,8,256,384]{3,2,1,0:T(8,128)(2,1)S(1)} %get-tuple-element.21) | copy-start | bytes 4718596
  104.6 3.5 %copy-start.12 = (f32[1024,384]{1,0:T(8,128)}, f32[1024,384]{1,0:T(8,128)S(1)}, u32[]{:S(2)}) copy-start(f32[1024,384]{1,0:T(8,128)S(1)} %fusion.41) | copy-start | bytes 4718596
  113.2 37.9 %copy-start.14 = (f32[2048]{0:T(1024)S(1)}, f32[2048]{0:T(1024)}, u32[]{:S(2)}) copy-start(f32[2048]{0:T(1024)} %param.13) | copy-start | bytes 24580
  113.2 37.9 %copy-start.3 = (bf16[128,2048]{1,0:T(8,128)(2,1)S(1)}, bf16[128,2048]{1,0:T(8,128)(2,1)}, u32[]{:S(2)}) copy-start(bf16[128,2048]{1,0:T(8,128)(2,1)} %param.11) | copy-start | bytes 1572868
  151.1 2.2 copy-start.1
  151.1 2.3 copy-start.5
  154.8 21.2 %copy-start.8 = (bf16[1,8,256,384]{3,2,1,0:T(8,128)(2,1)S(1)}, bf16[1,8,256,384]{3,2,1,0:T(8,128)(2,1)}, u32[]{:S(2)}) copy-start(bf16[1,8,256,384]{3,2,1,0:T(8,128)(2,1)} %copy-done.7) | copy-start | bytes 4718596
  173.5 2.6 %copy-start = (bf16[4,2,64,2048]{3,2,1,0:T(8,128)(2,1)S(1)}, bf16[4,2,64,2048]{3,2,1,0:T(8,128)(2,1)}, u32[]{:S(2)}) copy-start(bf16[4,2,64,2048]{3,2,1,0:T(8,128)(2,1)} %shard_map.114) | copy-start | bytes 6291460
  187.7 27.2 %copy-start.17 = (bf16[4,4,128,384]{3,2,1,0:T(8,128)(2,1)S(1)}, bf16[4,4,128,384]{3,2,1,0:T(8,128)(2,1)}, u32[]{:S(2)}) copy-start(bf16[4,4,128,384]{3,2,1,0:T(8,128)(2,1)} %get-tuple-element.14) | copy-start | bytes 4718596
  214.9 2.1 copy-start.16
  239.4 1.7 copy-start.2
  239.4 1.6 copy-start.6
  239.4 1.6 copy-start.13
  241.0 1.0 copy-start.4

commit v2 on v0

v2 whole, which is shorter than its diff:
```python
import functools
import itertools

import jax
import jax.numpy as jnp
from jax import lax
from jax.experimental import pallas as pl
from jax.experimental.pallas import tpu as pltpu
from jax.sharding import PartitionSpec as P

eps = 1e-06
F32, BF16 = jnp.float32, jnp.bfloat16
VMEM = pl.BlockSpec(memory_space=pltpu.VMEM)
DMA = pltpu.SemaphoreType.DMA


class Grid:
    def __init__(self, sizes):
        self.R, self.fs, self.tp = sizes
        self.fy = 2
        self.fz = self.fs // self.fy
        self.G = self.R * self.fy
        self.offsets = list(itertools.product(range(self.R), range(self.fy)))[1:]
        self.r, f, self.k = (lax.axis_index(n) for n in ("rep", "fs", "tp"))
        self.z, self.y = lax.div(f, self.fy), lax.rem(f, self.fy)
        self.g = self.r * self.fy + self.y

    def moved(self, o, sign=1):
        dr, dy = self.offsets[o]
        r = lax.rem(self.r + self.R + sign * dr, self.R)
        y = lax.rem(self.y + self.fy + sign * dy, self.fy)
        return r, y

    def index(self, o, sign=1):
        r, y = self.moved(o, sign)
        return r * self.fy + y

    def peer(self, o):
        r, y = self.moved(o)
        return {"rep": r, "fs": self.z * self.fy + y, "tp": self.k}

    def sibling_index(self, j):
        return lax.rem(self.k + j, self.tp)

    def sibling(self, j):
        return {"rep": self.r, "fs": self.z * self.fy + self.y, "tp": self.sibling_index(j)}

    def along(self, step):
        return lax.rem(self.z + self.fz + step, self.fz)

    def level(self, step):
        return {"rep": self.r, "fs": self.along(step) * self.fy + self.y, "tp": self.k}

    def barrier(self, group=False, pair=False, ring=False, levels=False):
        sem = pltpu.get_barrier_semaphore()
        targets = []
        if group:
            targets += [self.peer(o) for o in range(len(self.offsets))]
        if pair:
            targets += [self.sibling(j) for j in range(1, self.tp)]
        if levels:
            targets += [self.level(s) for s in range(1, self.fz)]
        elif ring:
            targets += [self.level(1), self.level(-1)]
        for t in targets:
            pl.semaphore_signal(sem, inc=1, device_id=t, device_id_type=pl.DeviceIdType.MESH)
        pl.semaphore_wait(sem, len(targets))


class Copies:
    def __init__(self, sems):
        self.sems, self.used = sems, 0

    def push(self, src, dst, to):
        copy = pltpu.make_async_remote_copy(
            src_ref=src, dst_ref=dst, send_sem=self.sems.at[0, self.used], recv_sem=self.sems.at[1, self.used],
            device_id=to, device_id_type=pl.DeviceIdType.MESH,
        )
        self.used += 1
        copy.start()
        return copy


class Ring:
    def __init__(self, m, cp, first, slot, chunks):
        self.m, self.cp, self.first, self.slot = m, cp, first, slot
        self.order = {0: chunks, 1: chunks[len(chunks) // 2:] + chunks[:len(chunks) // 2]}
        self.fronts = {0: set(chunks[: len(chunks) // 2]), 1: set(chunks[len(chunks) // 2:])}
        self.half = m.fz // 2
        self.sent, self.arrived = {}, set()

    def send(self, d, s, c):
        sign = 1 if d == 0 else -1
        block = self.m.along(-sign * (s - 1))
        src = self.first(c) if s == 1 else self.slot(block, c)
        self.sent[d, s, c] = self.cp.push(src, self.slot(block, c), self.m.level(sign))

    def arrive(self, d, s, c):
        if (d, s, c) not in self.sent or (d, s, c) in self.arrived:
            return
        self.sent[d, s, c].wait_recv()
        self.arrived.add((d, s, c))
        if s + 1 < self.half or (s + 1 == self.half and c in self.fronts[d]):
            self.send(d, s + 1, c)

    def step(self, s, ds=(0, 1)):
        for i in range(len(self.order[0])):
            for d in ds:
                self.arrive(d, s, self.order[d][i])

    def finish(self):
        for copy in self.sent.values():
            copy.wait_send()


def stages(m):
    half = m.fz // 2
    out = [(0, 0, ())]
    for s in range(1, half):
        out += [(-s, s, (0,)), (s, s, (1,))]
    return out + [(half, half, (0, 1))]


class Scatter:
    def __init__(self, m, cp, p, rx, tx, rg, acc):
        self.m, self.cp, self.p, self.rx, self.tx, self.rg, self.acc = m, cp, p, rx, tx, rg, acc
        self.pair, self.far = {}, {}

    def start(self, t):
        m = self.m
        for j in range(1, m.tp):
            src = self.p.at[t, :, :, m.sibling_index(j)]
            self.pair[t, j] = self.cp.push(src, self.rx.at[j - 1, t], m.sibling(j))

    def middle(self, t):
        m, n = self.m, len(self.m.offsets)
        for j in range(1, m.tp):
            self.pair[t, j].wait_recv()

        def total(block):
            value = self.p[t, :, block, m.k].astype(F32)
            for j in range(1, m.tp):
                value = value + self.rx[j - 1, t, :, block].astype(F32)
            return value

        for o in range(n):
            self.tx[t, o] = total(m.index(o)).astype(BF16)
            self.far[t, o] = self.cp.push(self.tx.at[t, o], self.rg.at[t, o], m.peer(o))
        self.acc[t] = total(m.g)

    def end(self, t):
        n = len(self.m.offsets)
        for o in range(n):
            self.far[t, o].wait_recv()
        value = self.acc[t]
        for o in range(n):
            value = value + self.rg[t, o].astype(F32)
        self.acc[t] = value

    def finish(self):
        for copy in list(self.pair.values()) + list(self.far.values()):
            copy.wait_send()


def flat(v):
    return v.reshape(-1, v.shape[-1])


def dot(a, b, ca, cb):
    return lax.dot_general(a, b, (((ca,), (cb,)), ((), ())), preferred_element_type=F32)


def kernel(sizes, D, w, x, dpost, branch_out, dnormed_out, owned_out,
           wout, xout, gate, up, hid, hout, p, rx, tx, rg, acc, dall, dhid, dgate, dup, dz,
           q, qx, qt, qg, dacc, dw, sems):
    m = Grid(sizes)
    cp = Copies(sems)
    n, fy, tp, fz = len(m.offsets), m.fy, m.tp, m.fz
    m.barrier(group=True, pair=True, levels=True)
    f = m.z * fy + m.y

    def where(z, c):
        e, i = c
        return wout.at[i, z * fy + lax.rem(m.y + e, fy)]

    def first(c):
        return w.at[m.g, c[1]] if c[0] == 0 else where(m.z, c)

    ys = {}

    def trade(i):
        for e in range(1, fy):
            o = m.offsets.index((0, e))
            ys[e, i] = cp.push(w.at[m.index(o), i], wout.at[i, f], m.peer(o))

    ring_a = Ring(m, cp, first, where, [(e, i) for i in (0, 1) for e in range(fy)])
    ring_b = Ring(m, cp, first, where, [(e, 2) for e in range(fy)])
    trade(0)
    trade(1)
    for i in (0, 1):
        ring_a.send(0, 1, (0, i))
        ring_a.send(1, 1, (0, 1 - i))
    xs = {o: cp.push(x.at[m.k], xout.at[m.g, m.k], m.peer(o)) for o in range(n)}
    trade(2)
    for i in range(3):
        wout[i, f] = w[m.g, i]
    xout[m.g] = x[...]
    for e in range(1, fy):
        back = (fy - e) % fy
        for i in (0, 1):
            ys[back, i].wait_recv()
        for i in (0, 1):
            ring_a.send(0, 1, (e, i))
            ring_a.send(1, 1, (e, 1 - i))
    for i in (0, 1):
        ring_a.arrive(0, 1, (0, i))
        ring_a.arrive(1, 1, (0, 1 - i))
    passed = []

    def spread(copies, out):
        for o in copies:
            copies[o].wait_recv()
            src = m.index(o, -1)
            for j in range(1, tp):
                passed.append(cp.push(out.at[src, m.k], out.at[src, m.k], m.sibling(j)))

    spread(xs, xout)
    ring_a.step(1)
    for e in range(fy):
        if e:
            ys[(fy - e) % fy, 2].wait_recv()
        for d in (0, 1):
            ring_b.send(d, 1, (e, 2))
    for copy in passed:
        copy.wait()
    passed.clear()

    gate[...] = jnp.zeros_like(gate)
    up[...] = jnp.zeros_like(up)
    for dist, s, ds in stages(m):
        for d in ds:
            ring_a.step(s, (d,))
        zt = m.along(dist)
        for e in range(fy):
            block = zt * fy + e

            def add(i, carry, block=block):
                rows = flat(xout[i, :, block])
                gate[i] += dot(rows, wout[0, block], 1, 0)
                up[i] += dot(rows, wout[1, block], 1, 0)
                return carry

            lax.fori_loop(0, m.G, add, 0)

    def activate(i, carry):
        v = gate[i]
        hid[i] = (v * (1.0 / (1.0 + jnp.exp(-v))) * up[i]).astype(BF16)
        return carry

    lax.fori_loop(0, m.G, activate, 0)
    ce = x.shape[2] // 2
    for t in range(tp):
        hout[m.z, t] = hid[:, (2 * t + 1) * ce:(2 * t + 2) * ce]
    ring_h = Ring(m, cp, lambda c: hout.at[m.z, c], lambda z, c: hout.at[z, c], list(range(tp)))

    sc = Scatter(m, cp, p, rx, tx, rg, acc)
    order = stages(m)
    for t, (dist, s, ds) in enumerate(order):
        for d in ds:
            ring_b.step(s, (d,))
        if t == len(order) - 1:
            for i in range(tp):
                for d in (0, 1):
                    ring_h.send(d, 1, ring_h.order[d][i])
        zt = m.along(dist)
        for e in range(fy):
            block = zt * fy + e

            def product(i, carry, block=block, e=e):
                p[t, e, i] = dot(hid[i], wout[2, block], 1, 1).astype(BF16).reshape(p.shape[3:])
                return carry

            lax.fori_loop(0, m.G, product, 0)
        sc.start(t)
        if t:
            sc.middle(t - 1)
    sc.middle(len(order) - 1)
    ssq = jnp.zeros((ce, 1), F32)
    mix = jnp.zeros((ce, 1), F32)
    for t, (dist, s, ds) in enumerate(order):
        sc.end(t)
        zt = m.along(dist)
        for e in range(fy):
            b = acc[t, e, ce:]
            ssq = ssq + jnp.sum(b * b, axis=-1, keepdims=True)
            mix = mix + jnp.sum(b * dpost[m.k, zt * fy + e], axis=-1, keepdims=True)
            branch_out[m.k, zt * fy + e] = acc[t, e, :ce]
    rz = lax.rsqrt(ssq / D + eps)
    factor = rz * rz * (mix / D)
    for t, (dist, s, ds) in enumerate(order):
        zt = m.along(dist)
        for e in range(fy):
            block = zt * fy + e
            dall[m.g, m.k, block] = (rz * (dpost[m.k, block] - acc[t, e, ce:] * factor)).astype(BF16)
    late = [cp.push(branch_out.at[m.k], branch_out.at[m.k], m.sibling(j)) for j in range(1, tp)]
    dg = {o: cp.push(dall.at[m.g, m.k], dall.at[m.g, m.k], m.peer(o)) for o in range(n)}
    own = [cp.push(dall.at[m.g, m.k], dall.at[m.g, m.k], m.sibling(j)) for j in range(1, tp)]
    ring_h.step(1)
    spread(dg, dall)
    across = {}
    for s in range(1, fz):
        src = dall.at[:, m.k, pl.ds(m.along(s) * fy, fy)]
        across[s] = cp.push(src, dz.at[m.z, m.k], m.level(s))
    for copy in passed + own:
        copy.wait()
    passed.clear()

    def back(i, carry):
        total = dot(flat(dall[i, :, 0]), wout[2, 0], 1, 0)
        for block in range(1, m.fs):
            total = total + dot(flat(dall[i, :, block]), wout[2, block], 1, 0)
        dhid[i] = total
        return carry

    lax.fori_loop(0, m.G, back, 0)

    def gates(i, carry):
        for t in range(tp):
            rows, mine = pl.ds((2 * t + 1) * ce, ce), pl.ds(t * ce, ce)
            g, dh = gate[i, rows], dhid[i, mine]
            sig = 1.0 / (1.0 + jnp.exp(-g))
            dgate[i, mine] = (dh * up[i, rows] * sig * (1.0 + g * (1.0 - sig))).astype(BF16)
            dup[i, mine] = (dh * g * sig).astype(BF16)
        return carry

    lax.fori_loop(0, m.G, gates, 0)
    dsc = Scatter(m, cp, q, qx, qt, qg, dacc)
    for t in range(fz):
        for e in range(fy):
            block = t * fy + e

            def terms(i, carry, block=block, e=e, t=t):
                v = dot(dgate[i], wout[0, block], 1, 1) + dot(dup[i], wout[1, block], 1, 1)
                q[t, e, i] = v.astype(BF16).reshape(q.shape[3:])
                return carry

            lax.fori_loop(0, m.G, terms, 0)
        dsc.start(t)
        if t:
            dsc.middle(t - 1)
    dsc.middle(fz - 1)
    for s in range(2, ring_h.half + 1):
        ring_h.step(s)
    dz[m.z] = jnp.stack([dall[:, t, pl.ds(m.z * fy, fy)] for t in range(tp)])
    for s in across:
        across[s].wait_recv()
        src = m.along(-s)
        for j in range(1, tp):
            passed.append(cp.push(dz.at[src, m.k], dz.at[src, m.k], m.sibling(j)))
    for t in range(fz):
        dsc.end(t)
        for e in range(fy):
            dnormed_out[m.k, t * fy + e] = dacc[t, e]
    last = [cp.push(dnormed_out.at[m.k], dnormed_out.at[m.k], m.sibling(j)) for j in range(1, tp)]
    for copy in passed:
        copy.wait()
    if fz == 1:
        ring_h.step(1)
    sends = []

    def gradient(r, e):
        a = dz[:, :, pl.ds(r * fy, fy), e]
        b = hout[:, :, pl.ds(r * fy, fy)]
        return dot(flat(a), flat(b), 0, 0).astype(BF16)

    for o in range(n):
        r, y = m.moved(o)
        dw[o] = gradient(r, y)
        sends.append(cp.push(dw.at[o], owned_out.at[m.g], m.peer(o)))
    owned_out[m.g] = gradient(m.r, m.y)
    for copy in sends + last + late:
        copy.wait()
    for copies in (xs, ys, dg, across):
        for copy in copies.values():
            copy.wait_send()
    for thing in (ring_a, ring_b, ring_h, sc, dsc):
        thing.finish()


def pre_norm(x, pre_gain):
    xf = x.astype(F32)
    scale = lax.rsqrt(jnp.mean(xf * xf, axis=-1, keepdims=True) + eps)
    return (xf, scale, (xf * scale * pre_gain).astype(BF16))


def body(sizes, x_late, x_early, cotangent, pre_gain, post_gain, gate_weight, up_weight, down_weight,
         down_grad_sum):
    R, fs, tp = sizes
    fy = 2
    fz, G = fs // fy, R * fy
    rows, D = x_late.shape
    drows, width = gate_weight.shape
    part = width // G
    n = G - 1
    ce = rows // tp
    c = 2 * ce
    S, V = jax.ShapeDtypeStruct, pltpu.VMEM

    late_f, late_rs, late_norm = pre_norm(x_late, pre_gain)
    early_f, early_rs, early_norm = pre_norm(x_early, pre_gain)
    blocks = lambda a: a.reshape(tp, ce, fs, drows).transpose(0, 2, 1, 3)
    rejoin = lambda a: a.transpose(0, 2, 1, 3).reshape(rows, D)
    normed = jnp.concatenate([blocks(late_norm), blocks(early_norm)], axis=2)
    weights = jnp.stack([w.reshape(drows, G, part) for w in (gate_weight, up_weight, down_weight)])
    weights = weights.transpose(2, 0, 1, 3)
    cot_f = cotangent.astype(F32)
    dpost = blocks(0.5 * cot_f * post_gain)
    ring = 2 * (fz // 2)
    count = (3 * (fy - 1) + ring * (3 * fy + tp) + 2 * (n + n * (tp - 1)) + 3 * (tp - 1)
             + 2 * fz * (tp - 1 + n) + (fz - 1) * tp + n)

    def scatter(c):
        return [
            V((fz, fy, G, tp, c, drows), BF16),
            V((tp - 1, fz, fy, G, c, drows), BF16),
            V((fz, n, fy, c, drows), BF16),
            V((fz, n, fy, c, drows), BF16),
            V((fz, fy, c, drows), F32),
        ]

    all_rows, early_rows = tp * c, tp * ce
    branch_l, dnormed, owned = pl.pallas_call(
        functools.partial(kernel, sizes, D),
        out_shape=[S((tp, fs, ce, drows), F32), S((tp, fs, ce, drows), F32), S((G, drows, part), BF16)],
        in_specs=[VMEM] * 3,
        out_specs=[VMEM] * 3,
        scratch_shapes=[
            V((3, fs, drows, part), BF16),
            V((G, tp, fs, c, drows), BF16),
            V((G, all_rows, part), F32),
            V((G, all_rows, part), F32),
            V((G, all_rows, part), BF16),
            V((fz, tp, G, ce, part), BF16),
        ] + scatter(c) + [
            V((G, tp, fs, ce, drows), BF16),
            V((G, early_rows, part), F32),
            V((G, early_rows, part), BF16),
            V((G, early_rows, part), BF16),
            V((fz, tp, G, fy, ce, drows), BF16),
        ] + scatter(ce) + [
            V((n, drows, part), BF16),
            DMA((2, count)),
        ],
        compiler_params=pltpu.CompilerParams(
            collective_id=0, has_side_effects=True, vmem_limit_bytes=60 * 1024 * 1024
        ),
    )(weights, normed, dpost)
    branch_l = rejoin(branch_l)
    late_rz = lax.rsqrt(jnp.mean(branch_l * branch_l, axis=-1, keepdims=True) + eps)
    y_late = (late_f + 0.5 * branch_l * late_rz * post_gain).astype(BF16)
    gained = pre_gain * rejoin(dnormed)
    dx_early = cot_f + early_rs * (
        gained - early_f * early_rs * early_rs * jnp.mean(early_f * gained, axis=-1, keepdims=True)
    )
    dx_early = dx_early.astype(BF16)
    owned = owned.transpose(1, 0, 2).reshape(drows, width)
    down_grad_out = down_grad_sum + owned.astype(F32)
    return (y_late, dx_early, down_grad_out)


def solution(mesh):
    sizes = tuple(mesh.shape[a] for a in ("rep", "fs", "tp"))
    in_specs = (
        P(("rep", "fs"), None),
        P(("rep", "fs"), None),
        P(("rep", "fs"), None),
        P(),
        P(),
        P("fs", "tp"),
        P("fs", "tp"),
        P("fs", "tp"),
        P(("rep", "fs"), "tp"),
    )
    out_specs = (P(("rep", "fs"), None), P(("rep", "fs"), None), P(("rep", "fs"), "tp"))
    return jax.shard_map(
        functools.partial(body, sizes), mesh=mesh, in_specs=in_specs, out_specs=out_specs, check_vma=False
    )
```

time: 442 us -> 178 us (0.40)
  waiting for transfers between devices: 380 us -> 0 us
  Pallas kernels: 0 us -> 149 us
  matrix products: 27.7 us -> 0 us
  between operations: 14.3 us -> 0.85 us
  local copies, waits for them, and re-layouts: 6.17 us -> 13.9 us
  starting transfers between devices: 6.17 us -> 0 us
    all_gather x4 -> x0, waiting for transfers between devices: 347 us -> none  [the longest x1 101 us: body(): lax.all_gather(gate_weight, 'fs', axis=0, tiled=True)]
    pallas_call x0 -> x1, Pallas kernels: none -> 149 us  [body(): pl.pallas_call(functools.partial(kernel, sizes, D), out_shape=[S((tp, fs,...]
    psum x2 -> x0, waiting for transfers between devices: 30 us -> none  [the longest x1 17.7 us: body(): lax.psum(partial_value.astype(jnp.bfloat16), 'tp').astype(jnp.float32)]
    dot_general x7 -> x0, matrix products: 27.7 us -> none  [the longest x3 10.7 us: right_product(): lax.dot_general(left, right, (((1,), (1,)), ((), ())), preferred_element_...]
    all_to_all x1 -> x0, starting transfers between devices: 5.93 us -> none  [body(): lax.all_to_all(dbranch, 'fs', split_axis=1, concat_axis=0, tiled=True)]
  transfers between devices with their start and end apart: 7 -> 0, of which waited for: 6 -> 0; matrix products, arithmetic and copies ran while one was open for 4% -> 0% of each run, Pallas kernels for 0% -> 0%
where the time goes in v2:
time: 178 us; the launch traced here: 175 us
  Pallas kernels  149 us (84%)
  local copies, waits for them, and re-layouts  13.9 us (8%)
  other arithmetic  10.7 us (6%)
    pallas_call x1, Pallas kernels, body(): pl.pallas_call(functools.partial(kernel, sizes, D), out_shape=[S((tp, fs,...  149 us
    unnamed x30, local copies, waits for them, and re-layouts  8.33 us

profile of v2, /device:TPU:0, one launch (start us, length us, event | category | flops | bytes accessed | tf_op | source)
XLA Modules:
  0.0 174.6 jit_solution(16766870755886097807)
XLA Ops:
  0.6 1.3 fusion.7
  1.9 1.2 fusion.11
  3.2 0.7 broadcast_multiply_fusion
  4.2 0.4 copy.15
  4.5 0.5 copy-done.5
  5.3 0.4 copy.16
  5.7 0.8 copy-done.6
  6.7 0.4 copy.17
  7.1 1.7 maximum_bitcast_fusion.w
  8.9 0.3 copy.28
  9.3 1.3 copy.34
  11.4 1.1 pad_maximum_fusion.x
  12.4 149.1 %shard_map.112 = (f32[2,8,64,256]{3,2,1,0:T(8,128)}, f32[2,8,64,256]{3,2,1,0:T(8,128)}, bf16[4,256,384]{2,1,0:T(8,128)(2,1)}) custom-call(bf16[4,3,256,384]{3,2,1,0:T(8,128)(2,1)} %maximum_bitcast_fusion.w, bf16[2,8,128,256]{3,2,1,0:T(8,128)(2,1)} %pad_maximum_fusion.x, f32[2,8,64,256]{3,2,1,0:T(8,128)} %bitcast.38), custom_call_target="tpu_custom_call" | custom-call | tf_op jit(solution)/shard_map/pallas_call | solution.py:432
  161.6 1.8 %copy.22 = f32[2,64,8,256]{3,2,1,0:T(8,128)S(1)} copy(f32[2,64,8,256]{3,1,2,0:T(8,128)} %bitcast.54) | data formatting | bytes 2097152 | tf_op jit(solution)/shard_map/transpose | solution.py:412
  163.4 0.3 copy.30
  164.0 1.2 fusion.6
  165.5 0.6 copy.21
  166.1 0.3 copy.29
  166.5 0.3 copy-done.9
  166.8 1.0 fusion.10
  167.9 0.5 copy.23
  168.4 3.0 %copy.24 = f32[256,1536]{0,1:T(8,128)} copy(f32[256,1536]{1,0:T(8,128)} %param.17) | data formatting | bytes 3145728 | tf_op args[8]
  171.4 1.6 bitcast_add_fusion
  173.0 1.6 copy.25
  (33 shorter events, 2.3 us)
Async XLA Ops:
  0.6 3.3 %copy-start.4 = (bf16[256,1536]{1,0:T(8,128)(2,1)S(1)}, bf16[256,1536]{1,0:T(8,128)(2,1)}, u32[]{:S(2)}) copy-start(bf16[256,1536]{1,0:T(8,128)(2,1)} %param.14) | copy-start | bytes 2359300
  3.9 1.1 copy-start.5
  5.3 1.1 copy-start.6
  7.1 1.7 copy-start.3
  9.3 1.3 copy-start
  9.3 1.3 copy-start.1
  9.3 1.3 copy-start.8
  164.0 1.2 copy-start.2
  166.1 0.7 copy-start.9
  166.4 1.4 copy-start.7

commit v3 on v2

--- a/solution.py
+++ b/solution.py
@@ -122,8 +122,9 @@
 
 
 class Scatter:
-    def __init__(self, m, cp, p, rx, tx, rg, acc):
+    def __init__(self, m, cp, p, rx, tx, rg, acc, place):
         self.m, self.cp, self.p, self.rx, self.tx, self.rg, self.acc = m, cp, p, rx, tx, rg, acc
+        self.place = place
         self.pair, self.far = {}, {}
 
     def start(self, t):
@@ -146,16 +147,16 @@
         for o in range(n):
             self.tx[t, o] = total(m.index(o)).astype(BF16)
             self.far[t, o] = self.cp.push(self.tx.at[t, o], self.rg.at[t, o], m.peer(o))
-        self.acc[t] = total(m.g)
+        self.acc[self.place(t)] = total(m.g)
 
     def end(self, t):
         n = len(self.m.offsets)
         for o in range(n):
             self.far[t, o].wait_recv()
-        value = self.acc[t]
+        value = self.acc[self.place(t)]
         for o in range(n):
             value = value + self.rg[t, o].astype(F32)
-        self.acc[t] = value
+        self.acc[self.place(t)] = value
 
     def finish(self):
         for copy in list(self.pair.values()) + list(self.far.values()):
@@ -170,28 +171,49 @@
     return lax.dot_general(a, b, (((ca,), (cb,)), ((), ())), preferred_element_type=F32)
 
 
-def kernel(sizes, D, w, x, dpost, branch_out, dnormed_out, owned_out,
-           wout, xout, gate, up, hid, hout, p, rx, tx, rg, acc, dall, dhid, dgate, dup, dz,
-           q, qx, qt, qg, dacc, dw, sems):
+def unit_scale(v):
+    return lax.rsqrt(jnp.mean(v * v, axis=-1, keepdims=True) + eps)
+
+
+def kernel(sizes, D, nw, *refs):
+    ws, refs = refs[:nw], refs[nw:]
+    (x_late, x_early, cot, pre_gain, post_gain, y_out, dx_out, owned_out,
+     wout, xout, dpost, gate, up, hid, hout, p, rx, tx, rg, acc, dall, dhid, dgate, dup, dz,
+           q, qx, qt, qg, dacc, dw, sems) = refs
     m = Grid(sizes)
     cp = Copies(sems)
     n, fy, tp, fz = len(m.offsets), m.fy, m.tp, m.fz
     m.barrier(group=True, pair=True, levels=True)
     f = m.z * fy + m.y
+    rows, part = x_late.shape[0], wout.shape[-1]
+    ce, drows = rows // tp, D // m.fs
+
+    def weight(g, i):
+        if nw == 1:
+            return ws[0].at[g, i]
+        return ws[i].at[:, pl.ds(pl.multiple_of(g * part, part), part)]
+
+    def owned_at(g):
+        if nw == 1:
+            return owned_out.at[g]
+        return owned_out.at[:, pl.ds(pl.multiple_of(g * part, part), part)]
+
+    def columns(block):
+        return slice(block * drows, (block + 1) * drows)
 
     def where(z, c):
         e, i = c
         return wout.at[i, z * fy + lax.rem(m.y + e, fy)]
 
     def first(c):
-        return w.at[m.g, c[1]] if c[0] == 0 else where(m.z, c)
+        return weight(m.g, c[1]) if c[0] == 0 else where(m.z, c)
 
     ys = {}
 
     def trade(i):
         for e in range(1, fy):
             o = m.offsets.index((0, e))
-            ys[e, i] = cp.push(w.at[m.index(o), i], wout.at[i, f], m.peer(o))
+            ys[e, i] = cp.push(weight(m.index(o), i), wout.at[i, f], m.peer(o))
 
     ring_a = Ring(m, cp, first, where, [(e, i) for i in (0, 1) for e in range(fy)])
     ring_b = Ring(m, cp, first, where, [(e, 2) for e in range(fy)])
@@ -200,11 +222,20 @@
     for i in (0, 1):
         ring_a.send(0, 1, (0, i))
         ring_a.send(1, 1, (0, 1 - i))
-    xs = {o: cp.push(x.at[m.k], xout.at[m.g, m.k], m.peer(o)) for o in range(n)}
+    for t in range(tp):
+        for place, ref in ((0, x_late), (ce, x_early)):
+            v = ref[t * ce:(t + 1) * ce].astype(F32)
+            v = (v * unit_scale(v) * pre_gain[...]).astype(BF16)
+            for block in range(m.fs):
+                xout[m.g, t, block, place:place + ce] = v[:, columns(block)]
+    for i in range(3):
+        wout[i, f] = weight(m.g, i)[...]
+    xs = {o: cp.push(xout.at[m.g, m.k], xout.at[m.g, m.k], m.peer(o)) for o in range(n)}
     trade(2)
-    for i in range(3):
-        wout[i, f] = w[m.g, i]
-    xout[m.g] = x[...]
+    mine = pl.ds(pl.multiple_of(m.k * ce, ce), ce)
+    v = 0.5 * cot[mine].astype(F32) * post_gain[...]
+    for block in range(m.fs):
+        dpost[block] = v[:, columns(block)]
     for e in range(1, fy):
         back = (fy - e) % fy
         for i in (0, 1):
@@ -258,13 +289,12 @@
         return carry
 
     lax.fori_loop(0, m.G, activate, 0)
-    ce = x.shape[2] // 2
     for t in range(tp):
         hout[m.z, t] = hid[:, (2 * t + 1) * ce:(2 * t + 2) * ce]
     ring_h = Ring(m, cp, lambda c: hout.at[m.z, c], lambda z, c: hout.at[z, c], list(range(tp)))
 
-    sc = Scatter(m, cp, p, rx, tx, rg, acc)
     order = stages(m)
+    sc = Scatter(m, cp, p, rx, tx, rg, acc, lambda t: m.along(order[t][0]))
     for t, (dist, s, ds) in enumerate(order):
         for d in ds:
             ring_b.step(s, (d,))
@@ -285,28 +315,28 @@
         if t:
             sc.middle(t - 1)
     sc.middle(len(order) - 1)
-    ssq = jnp.zeros((ce, 1), F32)
-    mix = jnp.zeros((ce, 1), F32)
-    for t, (dist, s, ds) in enumerate(order):
+    for t in range(len(order)):
         sc.end(t)
-        zt = m.along(dist)
-        for e in range(fy):
-            b = acc[t, e, ce:]
-            ssq = ssq + jnp.sum(b * b, axis=-1, keepdims=True)
-            mix = mix + jnp.sum(b * dpost[m.k, zt * fy + e], axis=-1, keepdims=True)
-            branch_out[m.k, zt * fy + e] = acc[t, e, :ce]
-    rz = lax.rsqrt(ssq / D + eps)
-    factor = rz * rz * (mix / D)
-    for t, (dist, s, ds) in enumerate(order):
-        zt = m.along(dist)
-        for e in range(fy):
-            block = zt * fy + e
-            dall[m.g, m.k, block] = (rz * (dpost[m.k, block] - acc[t, e, ce:] * factor)).astype(BF16)
-    late = [cp.push(branch_out.at[m.k], branch_out.at[m.k], m.sibling(j)) for j in range(1, tp)]
+    places = [divmod(block, fy) for block in range(m.fs)]
+
+    def row_sum(term):
+        return sum(jnp.sum(term(*place), axis=-1, keepdims=True) for place in places)
+
+    rz = lax.rsqrt(row_sum(lambda t, e: acc[t, e, ce:] * acc[t, e, ce:]) / D + eps)
+    mix = row_sum(lambda t, e: acc[t, e, ce:] * dpost[t * fy + e]) / D
+    factor = rz * rz * mix
+    for t, e in places:
+        dall[m.g, m.k, t * fy + e] = (rz * (dpost[t * fy + e] - acc[t, e, ce:] * factor)).astype(BF16)
     dg = {o: cp.push(dall.at[m.g, m.k], dall.at[m.g, m.k], m.peer(o)) for o in range(n)}
     own = [cp.push(dall.at[m.g, m.k], dall.at[m.g, m.k], m.sibling(j)) for j in range(1, tp)]
     ring_h.step(1)
+    late_rz = lax.rsqrt(row_sum(lambda t, e: acc[t, e, :ce] * acc[t, e, :ce]) / D + eps)
+    for t, e in places:
+        cols = columns(t * fy + e)
+        v = 0.5 * acc[t, e, :ce] * late_rz * post_gain[:, cols]
+        y_out[m.k, :, cols] = (x_late[mine, cols].astype(F32) + v).astype(BF16)
     spread(dg, dall)
+    late = [cp.push(y_out.at[m.k], y_out.at[m.k], m.sibling(j)) for j in range(1, tp)]
     across = {}
     for s in range(1, fz):
         src = dall.at[:, m.k, pl.ds(m.along(s) * fy, fy)]
@@ -326,15 +356,15 @@
 
     def gates(i, carry):
         for t in range(tp):
-            rows, mine = pl.ds((2 * t + 1) * ce, ce), pl.ds(t * ce, ce)
-            g, dh = gate[i, rows], dhid[i, mine]
+            its, to = pl.ds((2 * t + 1) * ce, ce), pl.ds(t * ce, ce)
+            g, dh = gate[i, its], dhid[i, to]
             sig = 1.0 / (1.0 + jnp.exp(-g))
-            dgate[i, mine] = (dh * up[i, rows] * sig * (1.0 + g * (1.0 - sig))).astype(BF16)
-            dup[i, mine] = (dh * g * sig).astype(BF16)
+            dgate[i, to] = (dh * up[i, its] * sig * (1.0 + g * (1.0 - sig))).astype(BF16)
+            dup[i, to] = (dh * g * sig).astype(BF16)
         return carry
 
     lax.fori_loop(0, m.G, gates, 0)
-    dsc = Scatter(m, cp, q, qx, qt, qg, dacc)
+    dsc = Scatter(m, cp, q, qx, qt, qg, dacc, lambda t: t)
     for t in range(fz):
         for e in range(fy):
             block = t * fy + e
@@ -359,13 +389,18 @@
             passed.append(cp.push(dz.at[src, m.k], dz.at[src, m.k], m.sibling(j)))
     for t in range(fz):
         dsc.end(t)
-        for e in range(fy):
-            dnormed_out[m.k, t * fy + e] = dacc[t, e]
-    last = [cp.push(dnormed_out.at[m.k], dnormed_out.at[m.k], m.sibling(j)) for j in range(1, tp)]
+    xf = x_early[mine].astype(F32)
+    rs = unit_scale(xf)
+    gained = lambda t, e: dacc[t, e] * pre_gain[:, columns(t * fy + e)]
+    mix = row_sum(lambda t, e: gained(t, e) * xf[:, columns(t * fy + e)]) / D
+    factor = rs * rs * mix
+    for t, e in places:
+        cols = columns(t * fy + e)
+        v = rs * (gained(t, e) - xf[:, cols] * factor)
+        dx_out[m.k, :, cols] = (cot[mine, cols].astype(F32) + v).astype(BF16)
+    last = [cp.push(dx_out.at[m.k], dx_out.at[m.k], m.sibling(j)) for j in range(1, tp)]
     for copy in passed:
         copy.wait()
-    if fz == 1:
-        ring_h.step(1)
     sends = []
 
     def gradient(r, e):
@@ -376,8 +411,8 @@
     for o in range(n):
         r, y = m.moved(o)
         dw[o] = gradient(r, y)
-        sends.append(cp.push(dw.at[o], owned_out.at[m.g], m.peer(o)))
-    owned_out[m.g] = gradient(m.r, m.y)
+        sends.append(cp.push(dw.at[o], owned_at(m.g), m.peer(o)))
+    owned_at(m.g)[...] = gradient(m.r, m.y)
     for copy in sends + last + late:
         copy.wait()
     for copies in (xs, ys, dg, across):
@@ -385,12 +420,6 @@
             copy.wait_send()
     for thing in (ring_a, ring_b, ring_h, sc, dsc):
         thing.finish()
-
-
-def pre_norm(x, pre_gain):
-    xf = x.astype(F32)
-    scale = lax.rsqrt(jnp.mean(xf * xf, axis=-1, keepdims=True) + eps)
-    return (xf, scale, (xf * scale * pre_gain).astype(BF16))
 
 
 def body(sizes, x_late, x_early, cotangent, pre_gain, post_gain, gate_weight, up_weight, down_weight,
@@ -406,15 +435,10 @@
     c = 2 * ce
     S, V = jax.ShapeDtypeStruct, pltpu.VMEM
 
-    late_f, late_rs, late_norm = pre_norm(x_late, pre_gain)
-    early_f, early_rs, early_norm = pre_norm(x_early, pre_gain)
-    blocks = lambda a: a.reshape(tp, ce, fs, drows).transpose(0, 2, 1, 3)
-    rejoin = lambda a: a.transpose(0, 2, 1, 3).reshape(rows, D)
-    normed = jnp.concatenate([blocks(late_norm), blocks(early_norm)], axis=2)
-    weights = jnp.stack([w.reshape(drows, G, part) for w in (gate_weight, up_weight, down_weight)])
-    weights = weights.transpose(2, 0, 1, 3)
-    cot_f = cotangent.astype(F32)
-    dpost = blocks(0.5 * cot_f * post_gain)
+    weights = [gate_weight, up_weight, down_weight]
+    aligned = part % 128 == 0
+    if not aligned:
+        weights = [jnp.stack([w.reshape(drows, G, part) for w in weights]).transpose(2, 0, 1, 3)]
     ring = 2 * (fz // 2)
     count = (3 * (fy - 1) + ring * (3 * fy + tp) + 2 * (n + n * (tp - 1)) + 3 * (tp - 1)
              + 2 * fz * (tp - 1 + n) + (fz - 1) * tp + n)
@@ -429,14 +453,18 @@
         ]
 
     all_rows, early_rows = tp * c, tp * ce
-    branch_l, dnormed, owned = pl.pallas_call(
-        functools.partial(kernel, sizes, D),
-        out_shape=[S((tp, fs, ce, drows), F32), S((tp, fs, ce, drows), F32), S((G, drows, part), BF16)],
-        in_specs=[VMEM] * 3,
+    y_late, dx_early, owned = pl.pallas_call(
+        functools.partial(kernel, sizes, D, len(weights)),
+        out_shape=[
+            S((tp, ce, D), BF16), S((tp, ce, D), BF16),
+            S((drows, width) if aligned else (G, drows, part), BF16),
+        ],
+        in_specs=[VMEM] * (len(weights) + 5),
         out_specs=[VMEM] * 3,
         scratch_shapes=[
             V((3, fs, drows, part), BF16),
             V((G, tp, fs, c, drows), BF16),
+            V((fs, ce, drows), F32),
             V((G, all_rows, part), F32),
             V((G, all_rows, part), F32),
             V((G, all_rows, part), BF16),
@@ -454,18 +482,11 @@
         compiler_params=pltpu.CompilerParams(
             collective_id=0, has_side_effects=True, vmem_limit_bytes=60 * 1024 * 1024
         ),
-    )(weights, normed, dpost)
-    branch_l = rejoin(branch_l)
-    late_rz = lax.rsqrt(jnp.mean(branch_l * branch_l, axis=-1, keepdims=True) + eps)
-    y_late = (late_f + 0.5 * branch_l * late_rz * post_gain).astype(BF16)
-    gained = pre_gain * rejoin(dnormed)
-    dx_early = cot_f + early_rs * (
-        gained - early_f * early_rs * early_rs * jnp.mean(early_f * gained, axis=-1, keepdims=True)
-    )
-    dx_early = dx_early.astype(BF16)
-    owned = owned.transpose(1, 0, 2).reshape(drows, width)
+    )(*weights, x_late, x_early, cotangent, pre_gain.reshape(1, D), post_gain.reshape(1, D))
+    if not aligned:
+        owned = owned.transpose(1, 0, 2).reshape(drows, width)
     down_grad_out = down_grad_sum + owned.astype(F32)
-    return (y_late, dx_early, down_grad_out)
+    return (y_late.reshape(rows, D), dx_early.reshape(rows, D), down_grad_out)
 
 
 def solution(mesh):

time: 178 us -> 157 us (0.88)
  local copies, waits for them, and re-layouts: 13.9 us -> 1.6 us
  other arithmetic: 10.7 us -> 2.55 us
    unnamed x30 -> x8, local copies, waits for them, and re-layouts: 8.33 us -> 1.6 us
    reduce_sum x4 -> x0, other arithmetic: 2.93 us -> none  [the longest x2 2.53 us: pre_norm(): scale = lax.rsqrt(jnp.mean(xf * xf, axis=-1, keepdims=True) + eps)]
    convert_element_type x4 -> x0, other arithmetic: 2.63 us -> none  [the longest x1 1.2 us: body(): dx_early = dx_early.astype(BF16)]
    transpose x2 -> x0, local copies, waits for them, and re-layouts: 2.45 us -> none  [body(): rejoin = lambda a: a.transpose(0, 2, 1, 3).reshape(rows, D)]
where the time goes in v3:
time: 157 us; the launch traced here: 154 us
  Pallas kernels  149 us (95%)
  other arithmetic  2.55 us (2%)
  local copies, waits for them, and re-layouts  1.6 us (1%)
    pallas_call x1, Pallas kernels, body(): pl.pallas_call(functools.partial(kernel, sizes, D, len(weights)), out_sha...  149 us

profile of v3, /device:TPU:0, one launch (start us, length us, event | category | flops | bytes accessed | tf_op | source)
XLA Modules:
  0.0 153.9 jit_solution(6591694985172417746)
XLA Ops:
  0.6 0.0 copy-start
  0.6 149.0 %shard_map.112 = (bf16[2,64,2048]{2,1,0:T(8,128)(2,1)}, bf16[2,64,2048]{2,1,0:T(8,128)(2,1)}, bf16[256,1536]{1,0:T(8,128)(2,1)}) custom-call(bf16[256,1536]{1,0:T(8,128)(2,1)} %refs_0_.1, bf16[256,1536]{1,0:T(8,128)(2,1)} %refs_1_.1, bf16[256,1536]{1,0:T(8,128)(2,1)} %refs_2_.1, bf16[128,2048]{1,0:T(8,128)(2,1)} %refs_3_.1, bf16[128,2048]{1,0:T(8,128)(2,1)} %refs_4_.1, ...), custom_call_target="tpu_custom_call" | custom-call | tf_op jit(solution)/shard_map/pallas_call | solution.py:456
  149.7 0.0 copy-done
  149.7 0.0 copy-start.2
  149.7 0.0 copy-start.1
  149.7 2.6 %convert_add_fusion = f32[256,1536]{1,0:T(8,128)} fusion(f32[256,1536]{1,0:T(8,128)S(1)} %copy-done, bf16[256,1536]{1,0:T(8,128)(2,1)} %get-tuple-element.8), kind=kLoop, calls=%fused_computation | loop fusion | flops 786432 | bytes 3932160 | tf_op jit(solution)/shard_map/add | solution.py:488
  152.3 0.0 copy-done.2
  152.3 0.8 copy.14
  153.1 0.0 copy-done.1
  153.1 0.8 copy.15
Async XLA Ops:
  0.6 149.1 %copy-start = (f32[256,1536]{1,0:T(8,128)S(1)}, f32[256,1536]{1,0:T(8,128)}, u32[]{:S(2)}) copy-start(f32[256,1536]{1,0:T(8,128)} %param.17) | copy-start | bytes 4718596
  149.7 2.6 %copy-start.2 = (bf16[2,64,2048]{2,1,0:T(8,128)(2,1)S(1)}, bf16[2,64,2048]{2,1,0:T(8,128)(2,1)}, u32[]{:S(2)}) copy-start(bf16[2,64,2048]{2,1,0:T(8,128)(2,1)} %get-tuple-element.6) | copy-start | bytes 1572868
  149.7 3.4 %copy-start.1 = (bf16[2,64,2048]{2,1,0:T(8,128)(2,1)S(1)}, bf16[2,64,2048]{2,1,0:T(8,128)(2,1)}, u32[]{:S(2)}) copy-start(bf16[2,64,2048]{2,1,0:T(8,128)(2,1)} %get-tuple-element.7) | copy-start | bytes 1572868

commit v4 on v3

--- a/solution.py
+++ b/solution.py
@@ -329,7 +329,11 @@
         dall[m.g, m.k, t * fy + e] = (rz * (dpost[t * fy + e] - acc[t, e, ce:] * factor)).astype(BF16)
     dg = {o: cp.push(dall.at[m.g, m.k], dall.at[m.g, m.k], m.peer(o)) for o in range(n)}
     own = [cp.push(dall.at[m.g, m.k], dall.at[m.g, m.k], m.sibling(j)) for j in range(1, tp)]
-    ring_h.step(1)
+    across = {}
+    for s in range(1, fz):
+        src = dall.at[m.g, m.k, pl.ds(m.along(s) * fy, fy)]
+        across[s] = cp.push(src, dz.at[m.z, m.k, m.g], m.level(s))
+    dz[m.z, m.k, m.g] = dall[m.g, m.k, pl.ds(m.z * fy, fy)]
     late_rz = lax.rsqrt(row_sum(lambda t, e: acc[t, e, :ce] * acc[t, e, :ce]) / D + eps)
     for t, e in places:
         cols = columns(t * fy + e)
@@ -337,10 +341,7 @@
         y_out[m.k, :, cols] = (x_late[mine, cols].astype(F32) + v).astype(BF16)
     spread(dg, dall)
     late = [cp.push(y_out.at[m.k], y_out.at[m.k], m.sibling(j)) for j in range(1, tp)]
-    across = {}
-    for s in range(1, fz):
-        src = dall.at[:, m.k, pl.ds(m.along(s) * fy, fy)]
-        across[s] = cp.push(src, dz.at[m.z, m.k], m.level(s))
+    ring_h.step(1)
     for copy in passed + own:
         copy.wait()
     passed.clear()
@@ -364,6 +365,9 @@
         return carry
 
     lax.fori_loop(0, m.G, gates, 0)
+    for s in across:
+        across[s].wait_recv()
+    feats = {o: cp.push(dz.at[:, m.k, m.g], dz.at[:, m.k, m.g], m.peer(o)) for o in range(n)}
     dsc = Scatter(m, cp, q, qx, qt, qg, dacc, lambda t: t)
     for t in range(fz):
         for e in range(fy):
@@ -381,12 +385,9 @@
     dsc.middle(fz - 1)
     for s in range(2, ring_h.half + 1):
         ring_h.step(s)
-    dz[m.z] = jnp.stack([dall[:, t, pl.ds(m.z * fy, fy)] for t in range(tp)])
-    for s in across:
-        across[s].wait_recv()
-        src = m.along(-s)
-        for j in range(1, tp):
-            passed.append(cp.push(dz.at[src, m.k], dz.at[src, m.k], m.sibling(j)))
+    for o in range(n):
+        feats[o].wait_recv()
+    passed += [cp.push(dz.at[:, m.k], dz.at[:, m.k], m.sibling(j)) for j in range(1, tp)]
     for t in range(fz):
         dsc.end(t)
     xf = x_early[mine].astype(F32)
@@ -415,7 +416,7 @@
     owned_at(m.g)[...] = gradient(m.r, m.y)
     for copy in sends + last + late:
         copy.wait()
-    for copies in (xs, ys, dg, across):
+    for copies in (xs, ys, dg, across, feats):
         for copy in copies.values():
             copy.wait_send()
     for thing in (ring_a, ring_b, ring_h, sc, dsc):
@@ -441,7 +442,7 @@
         weights = [jnp.stack([w.reshape(drows, G, part) for w in weights]).transpose(2, 0, 1, 3)]
     ring = 2 * (fz // 2)
     count = (3 * (fy - 1) + ring * (3 * fy + tp) + 2 * (n + n * (tp - 1)) + 3 * (tp - 1)
-             + 2 * fz * (tp - 1 + n) + (fz - 1) * tp + n)
+             + 2 * fz * (tp - 1 + n) + fz - 1 + n + tp - 1 + n)
 
     def scatter(c):
         return [

time: 157 us -> 161 us (1.025); the launches traced: 154 us -> 161 us
  Pallas kernels: 149 us -> 156 us
    pallas_call x1, Pallas kernels: 149 us -> 156 us  [body(): pl.pallas_call(functools.partial(kernel, sizes, D, len(weights)), out_sha...]
where the time goes in v4:
time: 161 us
  Pallas kernels  156 us (97%)
  other arithmetic  2.55 us (2%)
    pallas_call x1, Pallas kernels, body(): pl.pallas_call(functools.partial(kernel, sizes, D, len(weights)), out_sha...  156 us

profile of v4, /device:TPU:0, one launch (start us, length us, event | category | flops | bytes accessed | tf_op | source)
XLA Modules:
  0.0 161.0 jit_solution(7910105223280182812)
XLA Ops:
  0.6 0.0 copy-start
  0.6 156.2 %shard_map.112 = (bf16[2,64,2048]{2,1,0:T(8,128)(2,1)}, bf16[2,64,2048]{2,1,0:T(8,128)(2,1)}, bf16[256,1536]{1,0:T(8,128)(2,1)}) custom-call(bf16[256,1536]{1,0:T(8,128)(2,1)} %refs_0_.1, bf16[256,1536]{1,0:T(8,128)(2,1)} %refs_1_.1, bf16[256,1536]{1,0:T(8,128)(2,1)} %refs_2_.1, bf16[128,2048]{1,0:T(8,128)(2,1)} %refs_3_.1, bf16[128,2048]{1,0:T(8,128)(2,1)} %refs_4_.1, ...), custom_call_target="tpu_custom_call" | custom-call | tf_op jit(solution)/shard_map/pallas_call | solution.py:457
  156.8 0.0 copy-done
  156.8 0.0 copy-start.2
  156.8 0.0 copy-start.1
  156.8 2.6 %convert_add_fusion = f32[256,1536]{1,0:T(8,128)} fusion(f32[256,1536]{1,0:T(8,128)S(1)} %copy-done, bf16[256,1536]{1,0:T(8,128)(2,1)} %get-tuple-element.8), kind=kLoop, calls=%fused_computation | loop fusion | flops 786432 | bytes 3932160 | tf_op jit(solution)/shard_map/add | solution.py:489
  159.4 0.0 copy-done.2
  159.4 0.8 copy.14
  160.2 0.0 copy-done.1
  160.2 0.8 copy.15
Async XLA Ops:
  0.6 156.2 %copy-start = (f32[256,1536]{1,0:T(8,128)S(1)}, f32[256,1536]{1,0:T(8,128)}, u32[]{:S(2)}) copy-start(f32[256,1536]{1,0:T(8,128)} %param.17) | copy-start | bytes 4718596
  156.8 2.6 %copy-start.2 = (bf16[2,64,2048]{2,1,0:T(8,128)(2,1)S(1)}, bf16[2,64,2048]{2,1,0:T(8,128)(2,1)}, u32[]{:S(2)}) copy-start(bf16[2,64,2048]{2,1,0:T(8,128)(2,1)} %get-tuple-element.6) | copy-start | bytes 1572868
  156.8 3.4 %copy-start.1 = (bf16[2,64,2048]{2,1,0:T(8,128)(2,1)S(1)}, bf16[2,64,2048]{2,1,0:T(8,128)(2,1)}, u32[]{:S(2)}) copy-start(bf16[2,64,2048]{2,1,0:T(8,128)(2,1)} %get-tuple-element.7) | copy-start | bytes 1572868

commit v5 on v4

--- a/solution.py
+++ b/solution.py
@@ -299,7 +299,7 @@
         for d in ds:
             ring_b.step(s, (d,))
         if t == len(order) - 1:
-            for i in range(tp):
+            for i in range(tp // 2):
                 for d in (0, 1):
                     ring_h.send(d, 1, ring_h.order[d][i])
         zt = m.along(dist)
@@ -333,6 +333,9 @@
     for s in range(1, fz):
         src = dall.at[m.g, m.k, pl.ds(m.along(s) * fy, fy)]
         across[s] = cp.push(src, dz.at[m.z, m.k, m.g], m.level(s))
+    for i in range(tp // 2, tp):
+        for d in (0, 1):
+            ring_h.send(d, 1, ring_h.order[d][i])
     dz[m.z, m.k, m.g] = dall[m.g, m.k, pl.ds(m.z * fy, fy)]
     late_rz = lax.rsqrt(row_sum(lambda t, e: acc[t, e, :ce] * acc[t, e, :ce]) / D + eps)
     for t, e in places:
@@ -341,10 +344,15 @@
         y_out[m.k, :, cols] = (x_late[mine, cols].astype(F32) + v).astype(BF16)
     spread(dg, dall)
     late = [cp.push(y_out.at[m.k], y_out.at[m.k], m.sibling(j)) for j in range(1, tp)]
-    ring_h.step(1)
     for copy in passed + own:
         copy.wait()
     passed.clear()
+    for s in across:
+        across[s].wait_recv()
+    feats = {o: cp.push(dz.at[:, m.k, m.g], dz.at[:, m.k, m.g], m.peer(o)) for o in range(n)}
+    for i in range(tp // 2):
+        for d in (0, 1):
+            ring_h.arrive(d, 1, ring_h.order[d][i])
 
     def back(i, carry):
         total = dot(flat(dall[i, :, 0]), wout[2, 0], 1, 0)
@@ -365,9 +373,7 @@
         return carry
 
     lax.fori_loop(0, m.G, gates, 0)
-    for s in across:
-        across[s].wait_recv()
-    feats = {o: cp.push(dz.at[:, m.k, m.g], dz.at[:, m.k, m.g], m.peer(o)) for o in range(n)}
+    ring_h.step(1)
     dsc = Scatter(m, cp, q, qx, qt, qg, dacc, lambda t: t)
     for t in range(fz):
         for e in range(fy):
@@ -388,6 +394,20 @@
     for o in range(n):
         feats[o].wait_recv()
     passed += [cp.push(dz.at[:, m.k], dz.at[:, m.k], m.sibling(j)) for j in range(1, tp)]
+    for copy in passed:
+        copy.wait()
+    sends = []
+
+    def gradient(r, e):
+        a = dz[:, :, pl.ds(r * fy, fy), e]
+        b = hout[:, :, pl.ds(r * fy, fy)]
+        return dot(flat(a), flat(b), 0, 0).astype(BF16)
+
+    for o in range(n):
+        r, y = m.moved(o)
+        dw[o] = gradient(r, y)
+        sends.append(cp.push(dw.at[o], owned_at(m.g), m.peer(o)))
+    owned_at(m.g)[...] = gradient(m.r, m.y)
     for t in range(fz):
         dsc.end(t)
     xf = x_early[mine].astype(F32)
@@ -400,20 +420,6 @@
         v = rs * (gained(t, e) - xf[:, cols] * factor)
         dx_out[m.k, :, cols] = (cot[mine, cols].astype(F32) + v).astype(BF16)
     last = [cp.push(dx_out.at[m.k], dx_out.at[m.k], m.sibling(j)) for j in range(1, tp)]
-    for copy in passed:
-        copy.wait()
-    sends = []
-
-    def gradient(r, e):
-        a = dz[:, :, pl.ds(r * fy, fy), e]
-        b = hout[:, :, pl.ds(r * fy, fy)]
-        return dot(flat(a), flat(b), 0, 0).astype(BF16)
-
-    for o in range(n):
-        r, y = m.moved(o)
-        dw[o] = gradient(r, y)
-        sends.append(cp.push(dw.at[o], owned_at(m.g), m.peer(o)))
-    owned_at(m.g)[...] = gradient(m.r, m.y)
     for copy in sends + last + late:
         copy.wait()
     for copies in (xs, ys, dg, across, feats):

time: 161 us -> 157 us (0.975)
  Pallas kernels: 156 us -> 152 us
    pallas_call x1, Pallas kernels: 156 us -> 152 us  [body(): pl.pallas_call(functools.partial(kernel, sizes, D, len(weights)), out_sha...]
where the time goes in v5:
time: 157 us
  Pallas kernels  152 us (97%)
  other arithmetic  2.55 us (2%)
  local copies, waits for them, and re-layouts  1.6 us (1%)
    pallas_call x1, Pallas kernels, body(): pl.pallas_call(functools.partial(kernel, sizes, D, len(weights)), out_sha...  152 us

profile of v5, /device:TPU:0, one launch (start us, length us, event | category | flops | bytes accessed | tf_op | source)
XLA Modules:
  0.0 156.9 jit_solution(12660553979774488634)
XLA Ops:
  0.6 0.0 copy-start
  0.6 152.1 %shard_map.112 = (bf16[2,64,2048]{2,1,0:T(8,128)(2,1)}, bf16[2,64,2048]{2,1,0:T(8,128)(2,1)}, bf16[256,1536]{1,0:T(8,128)(2,1)}) custom-call(bf16[256,1536]{1,0:T(8,128)(2,1)} %refs_0_.1, bf16[256,1536]{1,0:T(8,128)(2,1)} %refs_1_.1, bf16[256,1536]{1,0:T(8,128)(2,1)} %refs_2_.1, bf16[128,2048]{1,0:T(8,128)(2,1)} %refs_3_.1, bf16[128,2048]{1,0:T(8,128)(2,1)} %refs_4_.1, ...), custom_call_target="tpu_custom_call" | custom-call | tf_op jit(solution)/shard_map/pallas_call | solution.py:463
  152.7 0.0 copy-done
  152.7 0.0 copy-start.2
  152.7 0.0 copy-start.1
  152.7 2.6 %convert_add_fusion = f32[256,1536]{1,0:T(8,128)} fusion(f32[256,1536]{1,0:T(8,128)S(1)} %copy-done, bf16[256,1536]{1,0:T(8,128)(2,1)} %get-tuple-element.8), kind=kLoop, calls=%fused_computation | loop fusion | flops 786432 | bytes 3932160 | tf_op jit(solution)/shard_map/add | solution.py:495
  155.3 0.0 copy-done.2
  155.3 0.8 copy.14
  156.1 0.0 copy-done.1
  156.1 0.8 copy.15
Async XLA Ops:
  0.6 152.1 %copy-start = (f32[256,1536]{1,0:T(8,128)S(1)}, f32[256,1536]{1,0:T(8,128)}, u32[]{:S(2)}) copy-start(f32[256,1536]{1,0:T(8,128)} %param.17) | copy-start | bytes 4718596
  152.7 2.6 %copy-start.2 = (bf16[2,64,2048]{2,1,0:T(8,128)(2,1)S(1)}, bf16[2,64,2048]{2,1,0:T(8,128)(2,1)}, u32[]{:S(2)}) copy-start(bf16[2,64,2048]{2,1,0:T(8,128)(2,1)} %get-tuple-element.6) | copy-start | bytes 1572868
  152.7 3.4 %copy-start.1 = (bf16[2,64,2048]{2,1,0:T(8,128)(2,1)S(1)}, bf16[2,64,2048]{2,1,0:T(8,128)(2,1)}, u32[]{:S(2)}) copy-start(bf16[2,64,2048]{2,1,0:T(8,128)(2,1)} %get-tuple-element.7) | copy-start | bytes 1572868
